TPU v7x, 32 devices: a whole 2x2x4 slice. The times are simulated.
32 devices in a mesh: sp: 4 (over y, x), tp: 8 (over z, core).
Axes of the slice: x: 2, y: 2, z: 4, core: 2. Of those that a mesh axis runs over, the one named last changes fastest.
Arguments:
- residual: bfloat16 [1536, 2048], P(('sp', 'tp')), may hold values from -40 to 40
- queries: bfloat16 [1536, 16, 256], P('sp', 'tp'), may hold values from -8.8 to 8.8
- query_rope: bfloat16 [1536, 16, 64], P('sp', 'tp'), may hold values from -72 to 72
- latent: bfloat16 [1536, 512], P('sp'), may hold values from -320 to 320
- key_rope: bfloat16 [1536, 32], P('sp'), may hold values from -48 to 48
- latent_gain: float32 [512], replicated, may hold values from 0.1 to 1.9
- key_weight: bfloat16 [512, 16, 256], P(None, 'tp'), may hold values from -0.25 to 0.25
- value_weight: bfloat16 [512, 16, 256], P(None, 'tp'), may hold values from -0.25 to 0.25
- out_weight: bfloat16 [16, 256, 2048], P('tp'), may hold values from -0.09375 to 0.09375
- norm_gain: float32 [2048], replicated, may hold values from 0.1 to 1.9
- routes: int32 [1536, 2], P('sp'), may hold values from 0 to 7, as said below
- group_gate: float32 [1536], P(('sp', 'tp')), may hold values from 0.5 to 1
- expert_share: float32 [1536, 2], P(('sp', 'tp')), may hold values from 0.2 to 1
- gate_weight: bfloat16 [8, 2048, 4096], P('sp', None, 'tp'), may hold values from -0.125 to 0.125
- up_weight: bfloat16 [8, 2048, 4096], P('sp', None, 'tp'), may hold values from -0.125 to 0.125
- down_weight: bfloat16 [8, 4096, 2048], P('sp', 'tp'), may hold values from -0.1875 to 0.1875
Outputs:
- layer_out: bfloat16 [1536, 2048], P(('sp', 'tp'))
Inputs may be any that keep to these rules, and one draw needn't show every extreme that they name: `routes`: each token names two different experts of one group; expert e belongs to group e // 2. In each aligned block of 48 tokens no expert is named more than 18 times, and one expert, the same in every block, is named exactly 18 times in every block.
All inputs are finite; a program needn't handle non-finite values.
Results may differ from a plain program's by a relative error of at most 0.025.
Values may be sent and summed in bfloat16 or wider, within the bound.
A program may use at most 64 MiB of HBM per device.

v0:
```python
import functools

import jax
import jax.numpy as jnp
from jax import lax
from jax.experimental import pallas as pl
from jax.experimental.pallas import tpu as pltpu
from jax.sharding import PartitionSpec as P

DK_A = 64
DV_A = 64
GROUPS = 4

rope_base = 10000.0
epsilon = 1e-06
floor_score = -1e30
MESH = pl.DeviceIdType.MESH
VM = pl.BlockSpec(memory_space=pltpu.VMEM)


def angle_tables(places, rope_width, repeats):
    steps = jnp.arange(repeats * rope_width // 2, dtype=jnp.int32) % (rope_width // 2)
    frequencies = rope_base ** (-(2 * steps).astype(jnp.float32) / rope_width)
    angles = places[:, None] * frequencies[None, :]
    return (jnp.cos(angles), jnp.sin(angles))


def rms_scale(values, gain_vector):
    values = values.astype(jnp.float32)
    inverse = lax.rsqrt(jnp.mean(values * values, axis=-1, keepdims=True) + epsilon)
    return values * inverse * gain_vector


def greet(targets):
    barrier = pltpu.get_barrier_semaphore()
    for target in targets:
        pl.semaphore_signal(barrier, inc=1, device_id=target, device_id_type=MESH)
    pl.semaphore_wait(barrier, len(targets))


def remote(src, dst, send, recv, target):
    return pltpu.make_async_remote_copy(
        src_ref=src,
        dst_ref=dst,
        send_sem=send,
        recv_sem=recv,
        device_id=target,
        device_id_type=MESH,
    )


def comm_call(kernel, out_shape, scratch, identity, args):
    return pl.pallas_call(
        kernel,
        out_shape=out_shape,
        in_specs=[VM] * len(args),
        out_specs=VM,
        scratch_shapes=scratch,
        compiler_params=pltpu.CompilerParams(
            collective_id=identity, has_side_effects=True, vmem_limit_bytes=48 * 1024 * 1024
        ),
    )(*args)


def greet_some(targets):
    barrier = pltpu.get_barrier_semaphore()
    count = 0
    for here, target in targets:

        @pl.when(here)
        def _():
            pl.semaphore_signal(barrier, inc=1, device_id=target, device_id_type=MESH)

        count = count + jnp.where(here, 1, 0)
    pl.semaphore_wait(barrier, count)


def line(tp_count):
    sp = lax.axis_index("sp")
    tp = lax.axis_index("tp")
    core = lax.rem(tp, 2)
    z = lax.div(tp, 2)
    depth = tp_count // 2
    partner = (sp, tp + 1 - 2 * core)
    return sp, core, z, depth, partner, (sp, tp + 2), (sp, tp - 2), z < depth - 1, z > 0


def expert_kernel(
    tp_count,
    x_ref,
    gate_ref,
    up_ref,
    down_ref,
    out_ref,
    held,
    gate,
    up,
    down,
    usend,
    dsend,
    psend,
    recv,
    wsem,
):
    sp, core, z, depth, partner, above, below, has_above, has_below = line(tp_count)
    tp = lax.axis_index("tp")
    experts = gate_ref.shape[0]
    model = gate_ref.shape[1]
    rows = x_ref.shape[0]
    middle = x_ref.shape[1] // 256 * 128
    parts = (slice(0, middle), slice(middle, x_ref.shape[1]))
    loads = [
        pltpu.make_async_copy(source, target, wsem.at[i])
        for i, (source, target) in enumerate(((gate_ref, gate), (up_ref, up), (down_ref, down)))
    ]
    for load in loads:
        load.start()
    greet_some([(True, partner), (has_above, above), (has_below, below)])

    def move(block, sems, place, part, target, source=None):
        source = held.at[block] if source is None else source
        return remote(
            source.at[:, parts[part]],
            held.at[block, :, parts[part]],
            sems.at[place, part],
            recv.at[block, part],
            target,
        )

    for part in range(2):

        @pl.when(has_above)
        def _():
            move(tp, usend, z, part, above, x_ref).start()

        @pl.when(has_below)
        def _():
            move(tp, dsend, z, part, below, x_ref).start()

        move(tp, psend, z, part, partner, x_ref).start()
    held[tp] = x_ref[...]

    def take(k):
        low, high = z - k, z + k
        for part in range(2):

            @pl.when(low >= 0)
            def _():
                block = low * 2 + core
                move(block, usend, low, part, partner).wait_recv()

                @pl.when(has_above)
                def _():
                    move(block, usend, low, part, above).start()

                move(block, psend, low, part, partner).start()

            @pl.when(high < depth)
            def _():
                block = high * 2 + core
                move(block, dsend, high, part, partner).wait_recv()

                @pl.when(has_below)
                def _():
                    move(block, dsend, high, part, below).start()

                move(block, psend, high, part, partner).start()

    def compute(place):
        for part in range(2):
            move(place * 2 + 1 - core, psend, place, part, partner).wait_recv()
        blocks = pl.ds(place * 2, 2)
        x = held[blocks].reshape(2 * rows, held.shape[2])
        inputs = x[:, :model]
        tail = x[:, model:].astype(jnp.float32)
        total = None
        for e in range(experts):
            scale = tail[:, e : e + 1] + tail[:, experts + e : experts + e + 1]
            gate_out = jnp.dot(inputs, gate[e], preferred_element_type=jnp.float32)
            up_out = jnp.dot(inputs, up[e], preferred_element_type=jnp.float32)
            hidden = (jax.nn.silu(gate_out) * up_out * scale).astype(inputs.dtype)
            part = jnp.dot(hidden, down[e], preferred_element_type=jnp.float32)
            total = part if e == 0 else total + part
        out_ref[blocks] = total.astype(out_ref.dtype).reshape(2, rows, model)

    if depth > 1:
        take(1)
    for load in loads:
        load.wait()

    side = jnp.where(z * 2 >= depth, -1, 1)

    def step(k, unused):
        one, two = z + side * k, z - side * k

        @pl.when((one >= 0) & (one < depth))
        def _():
            compute(one)

        @pl.when((k > 0) & (k + 1 < depth))
        def _():
            take(k + 1)

        @pl.when((k > 0) & (two >= 0) & (two < depth))
        def _():
            compute(two)

        return unused

    lax.fori_loop(0, depth, step, 0)
    for place in range(depth):
        for part in range(2):

            @pl.when(has_above & (place <= z))
            def _():
                move(place * 2 + core, usend, place, part, above).wait_send()

            @pl.when(has_below & (place >= z))
            def _():
                move(place * 2 + core, dsend, place, part, below).wait_send()

            move(place * 2 + core, psend, place, part, partner).wait_send()


def experts_over_tp(x, gate_weight, up_weight, down_weight, tp_count, identity):
    dma = pltpu.SemaphoreType.DMA
    depth = tp_count // 2
    model = gate_weight.shape[1]
    anywhere = pl.BlockSpec(memory_space=pl.ANY)
    return pl.pallas_call(
        functools.partial(expert_kernel, tp_count),
        out_shape=jax.ShapeDtypeStruct((tp_count, x.shape[0], model), x.dtype),
        in_specs=[VM, anywhere, anywhere, anywhere],
        out_specs=VM,
        scratch_shapes=[
            pltpu.VMEM((tp_count,) + x.shape, x.dtype),
            pltpu.VMEM(gate_weight.shape, gate_weight.dtype),
            pltpu.VMEM(up_weight.shape, up_weight.dtype),
            pltpu.VMEM(down_weight.shape, down_weight.dtype),
            dma((depth, 2)),
            dma((depth, 2)),
            dma((depth, 2)),
            dma((tp_count, 2)),
            dma((3,)),
        ],
        compiler_params=pltpu.CompilerParams(
            collective_id=identity, has_side_effects=True, vmem_limit_bytes=48 * 1024 * 1024
        ),
    )(x, gate_weight, up_weight, down_weight)


def reduce_tp_kernel(
    tp_count, x_ref, out_ref, partner_in, stage, up_in, down_in, send, recv, zsend, urecv, drecv
):
    sp, core, z, depth, partner, above, below, has_above, has_below = line(tp_count)
    greet_some([(True, partner), (has_above, above), (has_below, below)])

    middle = x_ref.shape[2] // 256 * 128
    parts = (slice(0, middle), slice(middle, x_ref.shape[2]))

    def swap(place, part):
        return remote(
            x_ref.at[place * 2 + 1 - core, :, parts[part]],
            partner_in.at[place, :, parts[part]],
            send.at[place, part],
            recv.at[place, part],
            partner,
        )

    def pass_on(place, part, arrivals, sems, target):
        return remote(
            stage.at[place, :, parts[part]],
            arrivals.at[place, :, parts[part]],
            zsend.at[place, part],
            sems.at[place, part],
            target,
        )

    def up(place, part):
        return pass_on(place, part, up_in, urecv, above)

    def down(place, part):
        return pass_on(place, part, down_in, drecv, below)

    def pair_sum(place, part):
        swap(place, part).wait_recv()
        mine = x_ref[place * 2 + core, :, parts[part]].astype(jnp.float32)
        return mine + partner_in[place, :, parts[part]].astype(jnp.float32)

    for j in range(depth):
        for part in range(2):
            swap(depth - 1 - j, part).start()
            if depth - 1 - j > j:
                swap(j, part).start()
        if depth - 1 - j <= j + 1:
            break

    for j in range(depth - 1):
        high, low = depth - 1 + z - j, j + z + 1 - depth
        for part in range(2):
            span = parts[part]

            @pl.when(z <= j)
            def _():
                stage[high, :, span] = pair_sum(high, part).astype(stage.dtype)

                @pl.when(has_below)
                def _():
                    up(high, part).wait_recv()
                    stage[high, :, span] = (
                        stage[high, :, span].astype(jnp.float32)
                        + up_in[high, :, span].astype(jnp.float32)
                    ).astype(stage.dtype)

                up(high, part).start()

            @pl.when(low >= 0)
            def _():
                stage[low, :, span] = pair_sum(low, part).astype(stage.dtype)

                @pl.when(has_above)
                def _():
                    down(low, part).wait_recv()
                    stage[low, :, span] = (
                        stage[low, :, span].astype(jnp.float32)
                        + down_in[low, :, span].astype(jnp.float32)
                    ).astype(stage.dtype)

                down(low, part).start()

    for part in range(2):
        span = parts[part]
        out_ref[:, span] = pair_sum(z, part)

        @pl.when(has_below)
        def _():
            up(z, part).wait_recv()
            out_ref[:, span] += up_in[z, :, span].astype(jnp.float32)

        @pl.when(has_above)
        def _():
            down(z, part).wait_recv()
            out_ref[:, span] += down_in[z, :, span].astype(jnp.float32)

    for place in range(depth):
        for part in range(2):
            swap(place, part).wait_send()

            @pl.when(place > z)
            def _():
                up(place, part).wait_send()

            @pl.when(place < z)
            def _():
                down(place, part).wait_send()


def reduce_tp(x, tp_count, identity):
    block = x.shape[1:]
    depth = tp_count // 2
    buffer = pltpu.VMEM((depth,) + block, x.dtype)
    return comm_call(
        functools.partial(reduce_tp_kernel, tp_count),
        jax.ShapeDtypeStruct(block, jnp.float32),
        [buffer] * 4 + [pltpu.SemaphoreType.DMA((depth, 2))] * 5,
        identity,
        (x,),
    )


def swap_sp_kernel(sp_count, x_ref, out_ref, send, recv, local_sem):
    me = lax.axis_index("sp")
    tp = lax.axis_index("tp")
    others = [lax.rem(me + k, sp_count) for k in range(1, sp_count)]
    greet([(other, tp) for other in others])
    copies = []
    for other in others:
        copy = remote(x_ref.at[other], out_ref.at[me], send.at[other], recv.at[me], (other, tp))
        copy.start()
        copies.append(copy)
    own = pltpu.make_async_copy(x_ref.at[me], out_ref.at[me], local_sem)
    own.start()
    own.wait()
    for other in others:
        remote(
            x_ref.at[other], out_ref.at[other], send.at[other], recv.at[other], (other, tp)
        ).wait_recv()
    for copy in copies:
        copy.wait_send()


def swap_sp(x, sp_count, identity):
    return comm_call(
        functools.partial(swap_sp_kernel, sp_count),
        jax.ShapeDtypeStruct(x.shape, x.dtype),
        [
            pltpu.SemaphoreType.DMA((sp_count,)),
            pltpu.SemaphoreType.DMA((sp_count,)),
            pltpu.SemaphoreType.DMA,
        ],
        identity,
        (x,),
    )


NT = (((1,), (1,)), ((), ()))


def attend_kernel(
    rope_width,
    sp_count,
    x_ref,
    q_ref,
    qr_ref,
    cos_ref,
    sin_ref,
    turn_ref,
    wk_ref,
    wv_ref,
    wo_ref,
    out_ref,
    turned,
    keys,
    values,
    tops,
    sums,
    acc,
    held,
    send,
    recv,
    fsend,
):
    me = lax.axis_index("sp")
    tp = lax.axis_index("tp")
    core = lax.rem(tp, 2)
    partner = (me, tp + 1 - 2 * core)
    tokens, width = q_ref.shape
    half = tokens // 2
    greet([(lax.rem(me + k, sp_count), tp) for k in range(1, sp_count)] + [partner])
    mine = pl.ds(pl.multiple_of(core * half, half), half)
    other = pl.ds(pl.multiple_of((1 - core) * half, half), half)

    def outgoing(to):
        return remote(
            x_ref.at[mine], held.at[me, mine], send.at[to], recv.at[me, core], (to, tp)
        )

    def incoming(source):
        return remote(
            x_ref.at[mine], held.at[source, mine], send.at[source], recv.at[source, core], partner
        )

    def forward(source):
        return remote(
            held.at[source, mine],
            held.at[source, mine],
            fsend.at[source],
            recv.at[source, core],
            partner,
        )

    def forwarded(source):
        return remote(
            held.at[source, other],
            held.at[source, other],
            fsend.at[source],
            recv.at[source, 1 - core],
            partner,
        )

    for to in reversed(range(sp_count)):

        @pl.when(to > me)
        def _():
            outgoing(to).start()

    latent = wk_ref.shape[0]
    pair_width = width // (qr_ref.shape[1] // (2 * rope_width))
    pairs = width // pair_width
    raw = qr_ref[...]
    swapped = jnp.dot(raw, turn_ref[...], preferred_element_type=jnp.float32)
    turned[...] = (raw.astype(jnp.float32) * cos_ref[...] + swapped * sin_ref[...]).astype(
        turned.dtype
    )
    scales = ((DK_A + rope_width) ** (-0.5), (pair_width - DK_A + rope_width) ** (-0.5))

    def block(index, first):
        compressed = x_ref[:, :latent] if first else held[index, :, :latent]
        rope = x_ref[:, latent:] if first else held[index, :, latent:]
        keys[...] = jnp.dot(compressed, wk_ref[...], preferred_element_type=jnp.float32).astype(
            keys.dtype
        )
        values[...] = jnp.dot(compressed, wv_ref[...], preferred_element_type=jnp.float32).astype(
            values.dtype
        )
        for pair in range(pairs):
            span = slice(pair * pair_width, (pair + 1) * pair_width)
            lane = lax.broadcasted_iota(jnp.int32, (tokens, pair_width), 1)
            rope_lane = lax.broadcasted_iota(jnp.int32, turned.shape, 1)
            factors, updates = [], []
            for group in range(2):
                head = pair * 2 + group
                chosen = (lane < DK_A) if group == 0 else (lane >= DK_A)
                query = jnp.where(chosen, q_ref[:, span], jnp.zeros((), q_ref.dtype))
                low = head * rope_width
                query_rope = jnp.where(
                    (rope_lane >= low) & (rope_lane < low + rope_width),
                    turned[...],
                    jnp.zeros((), turned.dtype),
                )
                scores = lax.dot_general(
                    query, keys[:, span], NT, preferred_element_type=jnp.float32
                ) + lax.dot_general(query_rope, rope, NT, preferred_element_type=jnp.float32)
                scores = scores * scales[group]
                if first:
                    row = lax.broadcasted_iota(jnp.int32, (tokens, tokens), 0)
                    column = lax.broadcasted_iota(jnp.int32, (tokens, tokens), 1)
                    scores = jnp.where(row >= column, scores, floor_score)
                    top = jnp.max(scores, axis=1, keepdims=True)
                else:
                    old = tops[head]
                    top = jnp.maximum(old, jnp.max(scores, axis=1, keepdims=True))
                    factors.append(jnp.exp(old - top))
                weights = jnp.exp(scores - top)
                total = jnp.sum(weights, axis=1, keepdims=True)
                tops[head] = top
                sums[head] = total if first else sums[head] * factors[-1] + total
                updates.append(
                    jnp.dot(
                        weights.astype(values.dtype),
                        values[:, span],
                        preferred_element_type=jnp.float32,
                    )
                )
            value_lane = lane < DV_A
            update = jnp.where(value_lane, updates[0], updates[1])
            if first:
                acc[:, span] = update
            else:
                acc[:, span] = (
                    acc[:, span] * jnp.where(value_lane, factors[0], factors[1]) + update
                )

    block(me, True)

    def step(i, unused):
        index = me - 1 - i
        incoming(index).wait_recv()
        forward(index).start()
        forwarded(index).wait_recv()
        block(index, False)
        return unused

    lax.fori_loop(0, me, step, 0)
    for pair in range(pairs):
        span = slice(pair * pair_width, (pair + 1) * pair_width)
        lane = lax.broadcasted_iota(jnp.int32, (tokens, pair_width), 1)
        bottom = jnp.where(lane < DV_A, sums[pair * 2], sums[pair * 2 + 1])
        keys[:, span] = (acc[:, span] / bottom).astype(keys.dtype)
    piece = 512
    for start in range(0, wo_ref.shape[1], piece):
        out_ref[:, start : start + piece] = jnp.dot(
            keys[...], wo_ref[:, start : start + piece], preferred_element_type=jnp.float32
        ).astype(out_ref.dtype)
    for place in range(sp_count):

        @pl.when(place < me)
        def _():
            forward(place).wait_send()

        @pl.when(place > me)
        def _():
            outgoing(place).wait_send()


def local(
    residual,
    queries,
    query_rope,
    latent,
    key_rope,
    latent_gain,
    key_weight,
    value_weight,
    out_weight,
    norm_gain,
    routes,
    group_gate,
    expert_share,
    gate_weight,
    up_weight,
    down_weight,
):
    tokens = queries.shape[0]
    pair_dev = queries.shape[1]
    sp_count = lax.axis_size("sp")
    tp_count = lax.axis_size("tp")
    row_count = tokens // tp_count
    rope_width = key_rope.shape[1]
    half = rope_width // 2
    copies = pair_dev * 2
    latent_width = latent.shape[1]
    model = residual.shape[1]
    low = jnp.bfloat16

    first_place = lax.axis_index("sp") * tokens
    places = (first_place + jnp.arange(tokens, dtype=jnp.int32)).astype(jnp.float32)
    cosine, sine = angle_tables(places, rope_width, 2 * copies)
    index = jnp.arange(copies * rope_width, dtype=jnp.int32)
    source = jnp.where(index % rope_width < half, index + half, index - half)
    sign = jnp.where(index % rope_width < half, -1.0, 1.0)
    turn = jnp.where(index[:, None] == source[None, :], sign[None, :], 0.0).astype(low)
    key_raw = jnp.tile(key_rope, (1, copies))
    rotated = (
        key_raw.astype(jnp.float32) * cosine
        + jnp.dot(key_raw, turn, preferred_element_type=jnp.float32) * sine
    ).astype(low)
    compressed = rms_scale(latent, latent_gain).astype(low)
    own_latent = jnp.concatenate([compressed, rotated], axis=1)

    width = pair_dev * queries.shape[2]
    scratch = [
        pltpu.VMEM((tokens, copies * rope_width), low),
        pltpu.VMEM((tokens, width), low),
        pltpu.VMEM((tokens, width), low),
        pltpu.VMEM((copies, tokens, 1), jnp.float32),
        pltpu.VMEM((copies, tokens, 1), jnp.float32),
        pltpu.VMEM((tokens, width), jnp.float32),
        pltpu.VMEM((sp_count,) + own_latent.shape, low),
        pltpu.SemaphoreType.DMA((sp_count,)),
        pltpu.SemaphoreType.DMA((sp_count, 2)),
        pltpu.SemaphoreType.DMA((sp_count,)),
    ]
    partial = pl.pallas_call(
        functools.partial(attend_kernel, rope_width, sp_count),
        out_shape=jax.ShapeDtypeStruct((tokens, model), low),
        in_specs=[VM] * 9,
        out_specs=VM,
        scratch_shapes=scratch,
        compiler_params=pltpu.CompilerParams(
            collective_id=0, has_side_effects=True, vmem_limit_bytes=48 * 1024 * 1024
        ),
    )(
        own_latent,
        queries.reshape(tokens, width),
        query_rope.reshape(tokens, copies * rope_width),
        cosine,
        sine,
        turn,
        key_weight.reshape(latent_width, -1),
        value_weight.reshape(latent_width, -1),
        out_weight.reshape(width, model),
    )
    head_total = reduce_tp(partial.reshape(tp_count, row_count, model), tp_count, 1)
    mixed_rows = residual.astype(jnp.float32) + head_total
    normed = rms_scale(mixed_rows, norm_gain).astype(low)

    experts_dev = gate_weight.shape[0]
    experts_all = experts_dev * sp_count
    top_count = routes.shape[1]
    capacity = max(2, 3 * row_count * top_count // (2 * experts_all))
    slots = experts_dev * capacity
    if experts_all // GROUPS == experts_dev == top_count:
        slots = capacity
    own = lax.dynamic_slice_in_dim(routes, lax.axis_index("tp") * row_count, row_count, 0)
    route_weight = group_gate[:, None] * expert_share / jnp.sum(expert_share, axis=1, keepdims=True)
    expert_ids = jnp.arange(experts_all, dtype=jnp.int32)
    named = own[:, :, None] == expert_ids[None, None, :]
    table = jnp.sum(jnp.where(named, route_weight[:, :, None], 0.0), axis=1)
    member = jnp.any(named, axis=1).reshape(row_count, sp_count, experts_dev).any(axis=2)
    counted = member.astype(jnp.int32)
    rank = jnp.cumsum(counted, axis=0) - counted
    slot_ids = jnp.arange(slots, dtype=jnp.int32)
    pick = (rank.T[:, None, :] == slot_ids[None, :, None]) & member.T[:, None, :]
    slot_weight = jnp.sum(
        jnp.where(
            pick[:, :, None, :],
            table.reshape(row_count, sp_count, experts_dev).transpose(1, 2, 0)[:, None],
            0.0,
        ),
        axis=3,
    )
    weight_high = slot_weight.astype(low)
    weight_low = (slot_weight - weight_high.astype(jnp.float32)).astype(low)
    pick_matrix = pick.astype(low).reshape(sp_count * slots, row_count)
    outgoing = jnp.dot(pick_matrix, normed, preferred_element_type=jnp.float32).astype(low)
    extra = jnp.concatenate([weight_high, weight_low], axis=2)
    extra = jnp.pad(extra, ((0, 0), (0, 0), (0, 128 - extra.shape[2])))
    outgoing = jnp.concatenate([outgoing.reshape(sp_count, slots, model), extra], axis=2)
    arrived = swap_sp(outgoing, sp_count, 2)
    rows = sp_count * slots
    expert_part = experts_over_tp(
        arrived.reshape(rows, model + 128), gate_weight, up_weight, down_weight, tp_count, 3
    )
    expert_out = reduce_tp(expert_part, tp_count, 4).astype(low)
    returned = swap_sp(expert_out.reshape(sp_count, slots, model), sp_count, 5)
    expert_mix = jnp.dot(
        pick_matrix.T, returned.reshape(rows, model), preferred_element_type=jnp.float32
    )
    return (mixed_rows + expert_mix).astype(low)


def solution(mesh):
    return jax.shard_map(
        local,
        mesh=mesh,
        in_specs=(
            P(("sp", "tp"), None),
            P("sp", "tp", None),
            P("sp", "tp", None),
            P("sp", None),
            P("sp", None),
            P(),
            P(None, "tp", None),
            P(None, "tp", None),
            P("tp", None, None),
            P(),
            P("sp", None),
            P(("sp", "tp")),
            P(("sp", "tp"), None),
            P("sp", None, "tp"),
            P("sp", None, "tp"),
            P("sp", "tp", None),
        ),
        out_specs=P(("sp", "tp"), None),
        check_vma=False,
    )
```

profile of v0, /device:TPU:0, one launch (start us, length us, event | category | flops | bytes accessed | tf_op | source)
XLA Modules:
  0.0 121.3 jit_solution(16425646856175885707)
XLA Ops:
  0.0 0.8 reduce_sum.47
  0.9 0.7 multiply_divide_fusion
  1.7 0.1 copy.67
  2.0 0.1 select_reduce_fusion
  2.1 0.3 copy.72
  2.4 0.1 copy.71
  2.5 0.1 copy.73
  2.6 0.1 copy.74
  2.8 0.1 fusion.15
  2.9 0.7 tile.4
  3.6 0.1 copy.64
  3.8 0.8 fusion.4
  4.6 1.2 fusion.5
  5.8 1.2 fusion.7
  7.0 1.1 copy.76
  8.1 0.1 copy.66.qr_ref
  8.2 0.8 multiply_sine_fusion
  9.0 1.1 copy.77
  10.1 1.1 copy.78
  11.3 14.6 %shard_map.154 = bf16[384,2048]{1,0:T(8,128)(2,1)S(1)} custom-call(bf16[384,640]{1,0:T(8,128)(2,1)S(1)} %pad_maximum_fusion.x_ref, bf16[384,512]{1,0:T(8,128)(2,1)S(1)} %bitcast.39, bf16[384,128]{1,0:T(8,128)(2,1)S(1)} %copy.66.qr_ref, f32[384,128]{1,0:T(8,128)S(1)} %get-tuple-element.6.cos_ref, f32[384,128]{1,0:T(8,128)S(1)} %get-tuple-element.5.sin_ref, ...), custom_call_target="tpu_custom_call" | custom-call | tf_op jit(solution)/shard_map/pallas_call | solution.py:634
  26.0 17.8 %shard_map.155 = f32[48,2048]{1,0:T(8,128)S(1)} custom-call(bf16[8,48,2048]{2,1,0:T(8,128)(2,1)S(1)} %bitcast.35), custom_call_target="tpu_custom_call" | custom-call | tf_op jit(solution)/shard_map/pallas_call | solution.py:53
  43.8 0.2 multiply_reduce_fusion
  44.0 0.1 eq.75
  44.1 0.3 convolution_convert_fusion
  44.4 0.1 reshape.117
  44.6 18.5 %shard_map.156 = bf16[4,18,2176]{2,1,0:T(8,128)(2,1)S(1)} custom-call(bf16[4,18,2176]{2,1,0:T(8,128)(2,1)S(1)} %pad_maximum_fusion.1.x_ref), custom_call_target="tpu_custom_call" | custom-call | tf_op jit(solution)/shard_map/pallas_call | solution.py:53
  63.0 0.1 reshape.119.x_ref
  63.1 26.6 %shard_map.157.x_ref = bf16[8,72,2048]{2,1,0:T(8,128)(2,1)S(1)} custom-call(bf16[72,2176]{1,0:T(8,128)(2,1)S(1)} %reshape.119.x_ref, bf16[2,2048,512]{2,1,0:T(8,128)(2,1)} %gate_ref.1, bf16[2,2048,512]{2,1,0:T(8,128)(2,1)} %up_ref.1, bf16[2,512,2048]{2,1,0:T(8,128)(2,1)} %down_ref.1), custom_call_target="tpu_custom_call" | custom-call | tf_op jit(solution)/shard_map/pallas_call | solution.py:230
  89.7 22.7 %shard_map.158 = f32[72,2048]{1,0:T(8,128)S(1)} custom-call(bf16[8,72,2048]{2,1,0:T(8,128)(2,1)S(1)} %shard_map.157.x_ref), custom_call_target="tpu_custom_call" | custom-call | tf_op jit(solution)/shard_map/pallas_call | solution.py:53
  112.4 0.1 reshape.120.x_ref
  112.5 7.8 %shard_map.159 = bf16[4,18,2048]{2,1,0:T(8,128)(2,1)S(1)} custom-call(bf16[4,18,2048]{2,1,0:T(8,128)(2,1)S(1)} %reshape.120.x_ref), custom_call_target="tpu_custom_call" | custom-call | tf_op jit(solution)/shard_map/pallas_call | solution.py:53
  120.4 0.9 fusion.1
  (38 shorter events, 0.6 us)
Async XLA Ops:
  0.0 1.5 %copy-start = (s32[384,2]{0,1:T(2,128)S(1)}, s32[384,2]{0,1:T(2,128)}, u32[]{:S(2)}) copy-start(s32[384,2]{0,1:T(2,128)} %param.26) | copy-start | bytes 9220
  0.0 8.1 %copy-start.3 = (bf16[384,2,64]{0,2,1:T(8,128)(2,1)S(1)}, bf16[384,2,64]{0,2,1:T(8,128)(2,1)}, u32[]{:S(2)}) copy-start(bf16[384,2,64]{0,2,1:T(8,128)(2,1)} %param.18) | copy-start | bytes 294916
  0.0 11.3 %copy-start.1 = (bf16[2,256,2048]{2,1,0:T(8,128)(2,1)S(1)}, bf16[2,256,2048]{2,1,0:T(8,128)(2,1)}, u32[]{:S(2)}) copy-start(bf16[2,256,2048]{2,1,0:T(8,128)(2,1)} %param.24) | copy-start | bytes 6291460
  11.3 32.5 %copy-start.2 = (bf16[48,2048]{1,0:T(8,128)(2,1)S(1)}, bf16[48,2048]{1,0:T(8,128)(2,1)}, u32[]{:S(2)}) copy-start(bf16[48,2048]{1,0:T(8,128)(2,1)} %param.16) | copy-start | bytes 589828
  11.3 32.8 %copy-start.4 = (f32[2048]{0:T(1024)S(1)}, f32[2048]{0:T(1024)}, u32[]{:S(2)}) copy-start(f32[2048]{0:T(1024)} %param.25) | copy-start | bytes 24580
where the time goes:
time: 122 us; the launch traced here: 121 us
  Pallas kernels  108 us (89%)
  local copies, waits for them, and re-layouts  5.62 us (5%)
  other arithmetic  5.31 us (4%)
  matrix products  2.07 us (2%)
    pallas_call x4, Pallas kernels, comm_call(): pl.pallas_call(kernel, out_shape=out_shape, in_specs=[VM] * len(args), ou...  66.8 us
    pallas_call x1, Pallas kernels, experts_over_tp(): pl.pallas_call(functools.partial(expert_kernel, tp_count), out_shape=jax....  26.6 us
    pallas_call x1, Pallas kernels, local(): pl.pallas_call(functools.partial(attend_kernel, rope_width, sp_count), ou...  14.6 us
    unnamed x13, local copies, waits for them, and re-layouts  3.33 us

commit v1 on v0

--- a/solution.py
+++ b/solution.py
@@ -85,168 +85,407 @@
     return sp, core, z, depth, partner, (sp, tp + 2), (sp, tp - 2), z < depth - 1, z > 0
 
 
-def expert_kernel(
+def moe_kernel(
+    sp_count,
     tp_count,
     x_ref,
+    pick_ref,
+    back_pick_ref,
     gate_ref,
     up_ref,
     down_ref,
     out_ref,
     held,
+    picked,
+    rows,
     gate,
     up,
     down,
+    result,
+    swapped,
+    summed,
+    back,
+    mixed,
+    stage,
+    up_in,
+    down_in,
     usend,
     dsend,
-    psend,
     recv,
+    ssend,
+    srecv,
+    fsend,
+    frecv,
+    wsend,
+    wrecv,
+    rsend,
+    rrecv,
+    zsend,
+    urecv,
+    drecv,
     wsem,
 ):
-    sp, core, z, depth, partner, above, below, has_above, has_below = line(tp_count)
+    me, core, z, depth, partner, above, below, has_above, has_below = line(tp_count)
     tp = lax.axis_index("tp")
     experts = gate_ref.shape[0]
     model = gate_ref.shape[1]
-    rows = x_ref.shape[0]
-    middle = x_ref.shape[1] // 256 * 128
-    parts = (slice(0, middle), slice(middle, x_ref.shape[1]))
+    tokens = x_ref.shape[0]
+    wide = x_ref.shape[1]
+    slots = rows.shape[3]
+    low = x_ref.dtype
+    gather_parts = (slice(0, wide // 256 * 128), slice(wide // 256 * 128, wide))
+    parts = (slice(0, model // 256 * 128), slice(model // 256 * 128, model))
+    others = [lax.rem(me + k, sp_count) for k in reversed(range(1, sp_count))]
     loads = [
         pltpu.make_async_copy(source, target, wsem.at[i])
         for i, (source, target) in enumerate(((gate_ref, gate), (up_ref, up), (down_ref, down)))
     ]
+    greet_some(
+        [(True, partner), (has_above, above), (has_below, below)]
+        + [(True, (other, tp)) for other in others]
+    )
+
+    def move(place, sems, part, target, source=None):
+        source = held.at[place] if source is None else source
+        return remote(
+            source.at[:, gather_parts[part]],
+            held.at[place, :, gather_parts[part]],
+            sems.at[place, part],
+            recv.at[place, part],
+            target,
+        )
+
+    for part in range(2):
+
+        @pl.when(has_above)
+        def _():
+            move(z, usend, part, above, x_ref).start()
+
+        @pl.when(has_below)
+        def _():
+            move(z, dsend, part, below, x_ref).start()
+
     for load in loads:
         load.start()
-    greet_some([(True, partner), (has_above, above), (has_below, below)])
-
-    def move(block, sems, place, part, target, source=None):
-        source = held.at[block] if source is None else source
-        return remote(
-            source.at[:, parts[part]],
-            held.at[block, :, parts[part]],
+    held[z] = x_ref[...]
+
+    def spread(place, other):
+        return remote(
+            picked.at[place, other],
+            rows.at[place, core, me],
+            ssend.at[place, other],
+            srecv.at[place, me],
+            (other, tp),
+        )
+
+    def spread_from(place, other):
+        return remote(
+            picked.at[place, other],
+            rows.at[place, core, other],
+            ssend.at[place, other],
+            srecv.at[place, other],
+            (other, tp),
+        )
+
+    def share(place, source):
+        return remote(
+            rows.at[place, core, source],
+            rows.at[place, core, source],
+            fsend.at[place, source],
+            frecv.at[place, source],
+            partner,
+        )
+
+    def share_own(place):
+        return remote(
+            picked.at[place, me],
+            rows.at[place, core, me],
+            fsend.at[place, me],
+            frecv.at[place, me],
+            partner,
+        )
+
+    def shared(place, source):
+        return remote(
+            rows.at[place, 1 - core, source],
+            rows.at[place, 1 - core, source],
+            fsend.at[place, source],
+            frecv.at[place, source],
+            partner,
+        )
+
+    def swap(place):
+        return remote(
+            result.at[place, 1 - core], swapped.at[place], wsend.at[place], wrecv.at[place], partner
+        )
+
+    def give(place, other):
+        return remote(
+            summed.at[place, other],
+            back.at[place, me],
+            rsend.at[place, other],
+            rrecv.at[place, me],
+            (other, tp),
+        )
+
+    def given(place, other):
+        return remote(
+            summed.at[place, other],
+            back.at[place, other],
+            rsend.at[place, other],
+            rrecv.at[place, other],
+            (other, tp),
+        )
+
+    def pass_on(place, part, arrivals, sems, target):
+        return remote(
+            stage.at[place, :, parts[part]],
+            arrivals.at[place, :, parts[part]],
+            zsend.at[place, part],
             sems.at[place, part],
-            recv.at[block, part],
             target,
         )
 
-    for part in range(2):
-
-        @pl.when(has_above)
-        def _():
-            move(tp, usend, z, part, above, x_ref).start()
-
-        @pl.when(has_below)
-        def _():
-            move(tp, dsend, z, part, below, x_ref).start()
-
-        move(tp, psend, z, part, partner, x_ref).start()
-    held[tp] = x_ref[...]
+    def rise(place, part):
+        return pass_on(place, part, up_in, urecv, above)
+
+    def fall(place, part):
+        return pass_on(place, part, down_in, drecv, below)
 
     def take(k):
-        low, high = z - k, z + k
+        lower, upper = z - k, z + k
         for part in range(2):
 
-            @pl.when(low >= 0)
-            def _():
-                block = low * 2 + core
-                move(block, usend, low, part, partner).wait_recv()
+            @pl.when((k > 0) & (lower >= 0))
+            def _():
+                move(lower, usend, part, below).wait_recv()
 
                 @pl.when(has_above)
                 def _():
-                    move(block, usend, low, part, above).start()
-
-                move(block, psend, low, part, partner).start()
-
-            @pl.when(high < depth)
-            def _():
-                block = high * 2 + core
-                move(block, dsend, high, part, partner).wait_recv()
+                    move(lower, usend, part, above).start()
+
+            @pl.when((k > 0) & (upper < depth))
+            def _():
+                move(upper, dsend, part, above).wait_recv()
 
                 @pl.when(has_below)
                 def _():
-                    move(block, dsend, high, part, below).start()
-
-                move(block, psend, high, part, partner).start()
+                    move(upper, dsend, part, below).start()
+
+    def choose(place):
+        chosen = jnp.dot(pick_ref[place], held[place], preferred_element_type=jnp.float32)
+        picked[place] = chosen.astype(low).reshape(sp_count, slots, wide)
+        for other in others:
+            spread(place, other).start()
+        share_own(place).start()
+        rows[place, core, me] = picked[place, me]
+
+    def relay(place):
+        for other in others:
+            spread_from(place, other).wait_recv()
+            share(place, other).start()
 
     def compute(place):
-        for part in range(2):
-            move(place * 2 + 1 - core, psend, place, part, partner).wait_recv()
-        blocks = pl.ds(place * 2, 2)
-        x = held[blocks].reshape(2 * rows, held.shape[2])
+        for source in range(sp_count):
+            shared(place, source).wait_recv()
+        x = rows[place].reshape(2 * sp_count * slots, wide)
         inputs = x[:, :model]
         tail = x[:, model:].astype(jnp.float32)
+        lane = lax.broadcasted_iota(jnp.int32, tail.shape, 1)
         total = None
         for e in range(experts):
-            scale = tail[:, e : e + 1] + tail[:, experts + e : experts + e + 1]
+            index = me * experts + e
+            here = (lane == index) | (lane == index + experts * sp_count)
+            scale = jnp.sum(jnp.where(here, tail, 0.0), axis=1, keepdims=True)
             gate_out = jnp.dot(inputs, gate[e], preferred_element_type=jnp.float32)
             up_out = jnp.dot(inputs, up[e], preferred_element_type=jnp.float32)
-            hidden = (jax.nn.silu(gate_out) * up_out * scale).astype(inputs.dtype)
+            hidden = (jax.nn.silu(gate_out) * up_out * scale).astype(low)
             part = jnp.dot(hidden, down[e], preferred_element_type=jnp.float32)
             total = part if e == 0 else total + part
-        out_ref[blocks] = total.astype(out_ref.dtype).reshape(2, rows, model)
-
-    if depth > 1:
-        take(1)
-    for load in loads:
-        load.wait()
-
-    side = jnp.where(z * 2 >= depth, -1, 1)
-
-    def step(k, unused):
-        one, two = z + side * k, z - side * k
-
-        @pl.when((one >= 0) & (one < depth))
-        def _():
-            compute(one)
-
-        @pl.when((k > 0) & (k + 1 < depth))
-        def _():
-            take(k + 1)
-
-        @pl.when((k > 0) & (two >= 0) & (two < depth))
-        def _():
-            compute(two)
-
+        result[place] = total.astype(low).reshape(2, sp_count, slots, model)
+        swap(place).start()
+
+    def settle(place):
+        swap(place).wait_recv()
+        both = result[place, core].astype(jnp.float32) + swapped[place].astype(jnp.float32)
+        summed[place] = both.astype(low)
+        for other in others:
+            give(place, other).start()
+        back[place, me] = summed[place, me]
+
+    def combine(place):
+        for other in others:
+            given(place, other).wait_recv()
+        mixed[place] = jnp.dot(
+            back_pick_ref[place],
+            back[place].reshape(sp_count * slots, model),
+            preferred_element_type=jnp.float32,
+        )
+        for part in range(2):
+            span = parts[part]
+
+            @pl.when((place > z) & (z == 0))
+            def _():
+                stage[place, :, span] = mixed[place, :, span].astype(low)
+                rise(place, part).start()
+
+            @pl.when((place < z) & (z == depth - 1))
+            def _():
+                stage[place, :, span] = mixed[place, :, span].astype(low)
+                fall(place, part).start()
+
+    def at(k, action):
+        def one(side, unused):
+            place = z + (1 - 2 * side) * k
+
+            @pl.when((place >= 0) & (place < depth) & ((k > 0) | (side == 0)) & (k >= 0))
+            def _():
+                action(place)
+
+            return unused
+
+        lax.fori_loop(0, 2, one, 0)
+
+    def step(t, unused):
+        @pl.when(t < depth)
+        def _():
+            take(t)
+            at(t, choose)
+
+        @pl.when(t == 1)
+        def _():
+            for load in loads:
+                load.wait()
+
+        at(t - 1, relay)
+        at(t - 2, settle)
+        at(t - 3, combine)
+        at(t - 1, compute)
         return unused
 
-    lax.fori_loop(0, depth, step, 0)
-    for place in range(depth):
+    lax.fori_loop(0, depth + 3, step, 0)
+
+    def hop(key, unused):
+        high = key - z
+        deep = 2 * depth - 2 - key - z
         for part in range(2):
+            span = parts[part]
+
+            @pl.when((high > z) & (high < depth) & has_below)
+            def _():
+                rise(high, part).wait_recv()
+                stage[high, :, span] = (
+                    mixed[high, :, span] + up_in[high, :, span].astype(jnp.float32)
+                ).astype(low)
+                rise(high, part).start()
+
+            @pl.when((deep >= 0) & (deep < z) & has_above)
+            def _():
+                fall(deep, part).wait_recv()
+                stage[deep, :, span] = (
+                    mixed[deep, :, span] + down_in[deep, :, span].astype(jnp.float32)
+                ).astype(low)
+                fall(deep, part).start()
+
+        return unused
+
+    lax.fori_loop(1, 2 * depth - 2, hop, 0)
+    for part in range(2):
+        span = parts[part]
+        out_ref[:, span] = mixed[z, :, span]
+
+        @pl.when(has_below)
+        def _():
+            rise(z, part).wait_recv()
+            out_ref[:, span] += up_in[z, :, span].astype(jnp.float32)
+
+        @pl.when(has_above)
+        def _():
+            fall(z, part).wait_recv()
+            out_ref[:, span] += down_in[z, :, span].astype(jnp.float32)
+
+    def finish(place, unused):
+        for part in range(2):
 
             @pl.when(has_above & (place <= z))
             def _():
-                move(place * 2 + core, usend, place, part, above).wait_send()
+                move(place, usend, part, above).wait_send()
 
             @pl.when(has_below & (place >= z))
             def _():
-                move(place * 2 + core, dsend, place, part, below).wait_send()
-
-            move(place * 2 + core, psend, place, part, partner).wait_send()
-
-
-def experts_over_tp(x, gate_weight, up_weight, down_weight, tp_count, identity):
+                move(place, dsend, part, below).wait_send()
+
+            @pl.when(place > z)
+            def _():
+                rise(place, part).wait_send()
+
+            @pl.when(place < z)
+            def _():
+                fall(place, part).wait_send()
+
+        for other in others:
+            spread(place, other).wait_send()
+            share(place, other).wait_send()
+            give(place, other).wait_send()
+        share_own(place).wait_send()
+        swap(place).wait_send()
+        return unused
+
+    lax.fori_loop(0, depth, finish, 0)
+
+
+def moe(x, pick, back_pick, gate_weight, up_weight, down_weight, sp_count, tp_count, identity):
     dma = pltpu.SemaphoreType.DMA
     depth = tp_count // 2
     model = gate_weight.shape[1]
+    tokens, wide = x.shape
+    slots = pick.shape[1] // sp_count
+    low = x.dtype
     anywhere = pl.BlockSpec(memory_space=pl.ANY)
+    each = dma((depth, sp_count))
+    two = dma((depth, 2))
+    block = pltpu.VMEM((depth, tokens, model), low)
+    group = pltpu.VMEM((depth, sp_count, slots, model), low)
     return pl.pallas_call(
-        functools.partial(expert_kernel, tp_count),
-        out_shape=jax.ShapeDtypeStruct((tp_count, x.shape[0], model), x.dtype),
-        in_specs=[VM, anywhere, anywhere, anywhere],
+        functools.partial(moe_kernel, sp_count, tp_count),
+        out_shape=jax.ShapeDtypeStruct((tokens, model), jnp.float32),
+        in_specs=[VM, VM, VM, anywhere, anywhere, anywhere],
         out_specs=VM,
         scratch_shapes=[
-            pltpu.VMEM((tp_count,) + x.shape, x.dtype),
+            pltpu.VMEM((depth, tokens, wide), low),
+            pltpu.VMEM((depth, sp_count, slots, wide), low),
+            pltpu.VMEM((depth, 2, sp_count, slots, wide), low),
             pltpu.VMEM(gate_weight.shape, gate_weight.dtype),
             pltpu.VMEM(up_weight.shape, up_weight.dtype),
             pltpu.VMEM(down_weight.shape, down_weight.dtype),
-            dma((depth, 2)),
-            dma((depth, 2)),
-            dma((depth, 2)),
-            dma((tp_count, 2)),
+            pltpu.VMEM((depth, 2, sp_count, slots, model), low),
+            group,
+            group,
+            group,
+            pltpu.VMEM((depth, tokens, model), jnp.float32),
+            block,
+            block,
+            block,
+            two,
+            two,
+            two,
+            each,
+            each,
+            each,
+            each,
+            dma((depth,)),
+            dma((depth,)),
+            each,
+            each,
+            two,
+            two,
+            two,
             dma((3,)),
         ],
         compiler_params=pltpu.CompilerParams(
-            collective_id=identity, has_side_effects=True, vmem_limit_bytes=48 * 1024 * 1024
+            collective_id=identity, has_side_effects=True, vmem_limit_bytes=60 * 1024 * 1024
         ),
-    )(x, gate_weight, up_weight, down_weight)
+    )(x, pick, back_pick, gate_weight, up_weight, down_weight)
 
 
 def reduce_tp_kernel(
@@ -363,41 +602,6 @@
         functools.partial(reduce_tp_kernel, tp_count),
         jax.ShapeDtypeStruct(block, jnp.float32),
         [buffer] * 4 + [pltpu.SemaphoreType.DMA((depth, 2))] * 5,
-        identity,
-        (x,),
-    )
-
-
-def swap_sp_kernel(sp_count, x_ref, out_ref, send, recv, local_sem):
-    me = lax.axis_index("sp")
-    tp = lax.axis_index("tp")
-    others = [lax.rem(me + k, sp_count) for k in range(1, sp_count)]
-    greet([(other, tp) for other in others])
-    copies = []
-    for other in others:
-        copy = remote(x_ref.at[other], out_ref.at[me], send.at[other], recv.at[me], (other, tp))
-        copy.start()
-        copies.append(copy)
-    own = pltpu.make_async_copy(x_ref.at[me], out_ref.at[me], local_sem)
-    own.start()
-    own.wait()
-    for other in others:
-        remote(
-            x_ref.at[other], out_ref.at[other], send.at[other], recv.at[other], (other, tp)
-        ).wait_recv()
-    for copy in copies:
-        copy.wait_send()
-
-
-def swap_sp(x, sp_count, identity):
-    return comm_call(
-        functools.partial(swap_sp_kernel, sp_count),
-        jax.ShapeDtypeStruct(x.shape, x.dtype),
-        [
-            pltpu.SemaphoreType.DMA((sp_count,)),
-            pltpu.SemaphoreType.DMA((sp_count,)),
-            pltpu.SemaphoreType.DMA,
-        ],
         identity,
         (x,),
     )
@@ -658,44 +862,42 @@
     experts_dev = gate_weight.shape[0]
     experts_all = experts_dev * sp_count
     top_count = routes.shape[1]
+    depth = tp_count // 2
     capacity = max(2, 3 * row_count * top_count // (2 * experts_all))
     slots = experts_dev * capacity
     if experts_all // GROUPS == experts_dev == top_count:
         slots = capacity
-    own = lax.dynamic_slice_in_dim(routes, lax.axis_index("tp") * row_count, row_count, 0)
+    slots = -(-slots // 8) * 8
+    tp = lax.axis_index("tp")
+    own = lax.dynamic_slice_in_dim(routes, tp * row_count, row_count, 0)
     route_weight = group_gate[:, None] * expert_share / jnp.sum(expert_share, axis=1, keepdims=True)
     expert_ids = jnp.arange(experts_all, dtype=jnp.int32)
     named = own[:, :, None] == expert_ids[None, None, :]
     table = jnp.sum(jnp.where(named, route_weight[:, :, None], 0.0), axis=1)
-    member = jnp.any(named, axis=1).reshape(row_count, sp_count, experts_dev).any(axis=2)
-    counted = member.astype(jnp.int32)
-    rank = jnp.cumsum(counted, axis=0) - counted
+    weight_high = table.astype(low)
+    weight_low = (table - weight_high.astype(jnp.float32)).astype(low)
+    extra = jnp.concatenate([weight_high, weight_low], axis=1)
+    extra = jnp.pad(extra, ((0, 0), (0, 128 - extra.shape[1])))
+
+    column = lax.dynamic_index_in_dim(
+        routes.reshape(depth, 2, row_count, top_count), lax.rem(tp, 2), 1, keepdims=False
+    )
+    goal = column // experts_dev
+    member = jnp.any(goal[:, :, :, None] == jnp.arange(sp_count, dtype=jnp.int32), axis=2)
+    row = jnp.arange(row_count, dtype=jnp.int32)
+    earlier = (row[:, None] > row[None, :]).astype(low)
+    rank = jnp.einsum(
+        "rq,zqs->zrs", earlier, member.astype(low), preferred_element_type=jnp.float32
+    )
+    rank = jnp.where(member, rank.astype(jnp.int32), -1)
     slot_ids = jnp.arange(slots, dtype=jnp.int32)
-    pick = (rank.T[:, None, :] == slot_ids[None, :, None]) & member.T[:, None, :]
-    slot_weight = jnp.sum(
-        jnp.where(
-            pick[:, :, None, :],
-            table.reshape(row_count, sp_count, experts_dev).transpose(1, 2, 0)[:, None],
-            0.0,
-        ),
-        axis=3,
-    )
-    weight_high = slot_weight.astype(low)
-    weight_low = (slot_weight - weight_high.astype(jnp.float32)).astype(low)
-    pick_matrix = pick.astype(low).reshape(sp_count * slots, row_count)
-    outgoing = jnp.dot(pick_matrix, normed, preferred_element_type=jnp.float32).astype(low)
-    extra = jnp.concatenate([weight_high, weight_low], axis=2)
-    extra = jnp.pad(extra, ((0, 0), (0, 0), (0, 128 - extra.shape[2])))
-    outgoing = jnp.concatenate([outgoing.reshape(sp_count, slots, model), extra], axis=2)
-    arrived = swap_sp(outgoing, sp_count, 2)
-    rows = sp_count * slots
-    expert_part = experts_over_tp(
-        arrived.reshape(rows, model + 128), gate_weight, up_weight, down_weight, tp_count, 3
-    )
-    expert_out = reduce_tp(expert_part, tp_count, 4).astype(low)
-    returned = swap_sp(expert_out.reshape(sp_count, slots, model), sp_count, 5)
-    expert_mix = jnp.dot(
-        pick_matrix.T, returned.reshape(rows, model), preferred_element_type=jnp.float32
+    back_pick = (rank[:, :, :, None] == slot_ids).astype(low)
+    back_pick = back_pick.reshape(depth, row_count, sp_count * slots)
+    pick = (jnp.swapaxes(rank, 1, 2)[:, :, None, :] == slot_ids[:, None]).astype(low)
+    pick = pick.reshape(depth, sp_count * slots, row_count)
+    x = jnp.concatenate([normed, extra], axis=1)
+    expert_mix = moe(
+        x, pick, back_pick, gate_weight, up_weight, down_weight, sp_count, tp_count, 3
     )
     return (mixed_rows + expert_mix).astype(low)
 

time: 122 us -> 121 us (level)
  Pallas kernels: 108 us -> 104 us
  other arithmetic: 5.31 us -> 8.82 us
    pallas_call x4 -> x1, Pallas kernels: 66.8 us -> 17.8 us  [comm_call(): pl.pallas_call(kernel, out_shape=out_shape, in_specs=[VM] * len(args), ou...]
    pallas_call x1, Pallas kernels: 26.6 us -> 71.4 us  [moe(): pl.pallas_call(functools.partial(moe_kernel, sp_count, tp_count), out_sha...]
    convert_element_type x3 -> x5, other arithmetic: 0.05 us -> 3.21 us  [the longest x1 1.72 us: local(): return (mixed_rows + expert_mix).astype(low)]
    unnamed x13 -> x11, local copies, waits for them, and re-layouts: 3.33 us -> 3.33 us
where the time goes in v1:
time: 121 us; the launch traced here: 120 us
  Pallas kernels  104 us (86%)
  other arithmetic  8.82 us (7%)
  local copies, waits for them, and re-layouts  6.36 us (5%)
    pallas_call x1, Pallas kernels, moe(): pl.pallas_call(functools.partial(moe_kernel, sp_count, tp_count), out_sha...  71.4 us
    pallas_call x1, Pallas kernels, comm_call(): pl.pallas_call(kernel, out_shape=out_shape, in_specs=[VM] * len(args), ou...  17.8 us
    pallas_call x1, Pallas kernels, local(): pl.pallas_call(functools.partial(attend_kernel, rope_width, sp_count), ou...  14.6 us
    unnamed x11, local copies, waits for them, and re-layouts  3.33 us

profile of v1, /device:TPU:0, one launch (start us, length us, event | category | flops | bytes accessed | tf_op | source)
XLA Modules:
  0.0 120.2 jit_solution(5608295510195668491)
XLA Ops:
  0.0 0.8 reduce_sum.38
  0.8 0.7 multiply_divide_fusion
  1.5 0.8 constant_dynamic-slice_fusion.1
  2.3 0.1 copy.52
  2.4 0.7 tile.4
  3.2 0.1 copy.49
  3.3 0.8 fusion.2
  4.2 1.2 fusion.3
  5.4 1.2 fusion.5
  6.6 1.1 copy.58
  7.6 1.0 copy.51.qr_ref
  8.7 0.8 multiply_sine_fusion
  9.4 1.1 copy.59
  10.6 1.1 copy.60
  11.7 0.0 copy-start.1
  11.7 0.0 copy-done
  11.7 0.0 copy-start.2
  11.7 0.0 copy-start.3
  11.8 14.6 %shard_map.154 = bf16[384,2048]{1,0:T(8,128)(2,1)S(1)} custom-call(bf16[384,640]{1,0:T(8,128)(2,1)S(1)} %pad_maximum_fusion.x_ref, bf16[384,512]{1,0:T(8,128)(2,1)S(1)} %bitcast.43, bf16[384,128]{1,0:T(8,128)(2,1)S(1)} %copy.51.qr_ref, f32[384,128]{1,0:T(8,128)S(1)} %get-tuple-element.8.cos_ref, f32[384,128]{1,0:T(8,128)S(1)} %get-tuple-element.7.sin_ref, ...), custom_call_target="tpu_custom_call" | custom-call | tf_op jit(solution)/shard_map/pallas_call | solution.py:838
  26.4 17.8 %shard_map.155 = f32[48,2048]{1,0:T(8,128)S(1)} custom-call(bf16[8,48,2048]{2,1,0:T(8,128)(2,1)S(1)} %bitcast.39), custom_call_target="tpu_custom_call" | custom-call | tf_op jit(solution)/shard_map/pallas_call | solution.py:53
  44.2 0.2 multiply_reduce_fusion
  44.4 0.0 copy-done.2
  44.4 0.1 multiply_convert_fusion
  44.5 0.7 fusion.7.x_ref
  45.2 0.1 eq.101
  45.3 0.1 reshape.126
  45.5 0.1 bitcast_select_fusion.1
  45.6 0.7 fusion.8.pick_ref
  46.4 0.1 copy.55
  46.5 0.6 compare_convert_fusion.back_pick_ref
  47.1 71.4 %shard_map.156 = f32[48,2048]{1,0:T(8,128)} custom-call(bf16[48,2176]{1,0:T(8,128)(2,1)} %fusion.7.x_ref, bf16[4,96,48]{2,1,0:T(8,128)(2,1)} %fusion.8.pick_ref, bf16[4,48,96]{2,1,0:T(8,128)(2,1)} %compare_convert_fusion.back_pick_ref, bf16[2,2048,512]{2,1,0:T(8,128)(2,1)} %gate_ref.1, bf16[2,2048,512]{2,1,0:T(8,128)(2,1)} %up_ref.1, ...), custom_call_target="tpu_custom_call" | custom-call | tf_op jit(solution)/shard_map/pallas_call | solution.py:449
  118.5 1.7 %add_convert_fusion = bf16[48,2048]{1,0:T(8,128)(2,1)} fusion(f32[48,2048]{1,0:T(8,128)} %shard_map.156, f32[48,2048]{1,0:T(8,128)S(1)} %shard_map.155, bf16[48,2048]{1,0:T(8,128)(2,1)S(1)} %copy-done.1), kind=kLoop, calls=%fused_computation.13 | loop fusion | flops 393216 | bytes 1179648 | tf_op jit(solution)/shard_map/convert_element_type | solution.py:902
  (21 shorter events, 0.2 us)
Async XLA Ops:
  0.0 11.7 %copy-start = (bf16[2,256,2048]{2,1,0:T(8,128)(2,1)S(1)}, bf16[2,256,2048]{2,1,0:T(8,128)(2,1)}, u32[]{:S(2)}) copy-start(bf16[2,256,2048]{2,1,0:T(8,128)(2,1)} %param.24) | copy-start | bytes 6291460
  11.7 32.5 %copy-start.1 = (bf16[48,2048]{1,0:T(8,128)(2,1)S(1)}, bf16[48,2048]{1,0:T(8,128)(2,1)}, u32[]{:S(2)}) copy-start(bf16[48,2048]{1,0:T(8,128)(2,1)} %param.16) | copy-start | bytes 589828
  11.7 32.7 %copy-start.2 = (f32[2048]{0:T(1024)S(1)}, f32[2048]{0:T(1024)}, u32[]{:S(2)}) copy-start(f32[2048]{0:T(1024)} %param.25) | copy-start | bytes 24580
  11.7 33.6 %copy-start.3 = (s32[384,2]{0,1:T(2,128)S(1)}, s32[384,2]{0,1:T(2,128)}, u32[]{:S(2)}) copy-start(s32[384,2]{0,1:T(2,128)} %param.26) | copy-start | bytes 9220

commit v2 on v1

v2 whole, which is shorter than its diff:
```python
import functools

import jax
import jax.numpy as jnp
from jax import lax
from jax.experimental import pallas as pl
from jax.experimental.pallas import tpu as pltpu
from jax.sharding import PartitionSpec as P

DK_A = 64
DV_A = 64
GROUPS = 4

rope_base = 10000.0
epsilon = 1e-06
floor_score = -1e30
MESH = pl.DeviceIdType.MESH
VM = pl.BlockSpec(memory_space=pltpu.VMEM)


def angle_tables(places, rope_width):
    steps = jnp.arange(rope_width // 2, dtype=jnp.int32)
    frequencies = rope_base ** (-(2 * steps).astype(jnp.float32) / rope_width)
    angles = places[None, :] * frequencies[:, None]
    return (jnp.cos(angles), jnp.sin(angles))


def rms_scale(values, gain_vector):
    values = values.astype(jnp.float32)
    inverse = lax.rsqrt(jnp.mean(values * values, axis=-1, keepdims=True) + epsilon)
    return values * inverse * gain_vector


def remote(src, dst, send, recv, target):
    return pltpu.make_async_remote_copy(
        src_ref=src,
        dst_ref=dst,
        send_sem=send,
        recv_sem=recv,
        device_id=target,
        device_id_type=MESH,
    )


def greet_some(targets):
    barrier = pltpu.get_barrier_semaphore()
    count = 0
    for here, target in targets:

        @pl.when(here)
        def _():
            pl.semaphore_signal(barrier, inc=1, device_id=target, device_id_type=MESH)

        count = count + jnp.where(here, 1, 0)
    pl.semaphore_wait(barrier, count)


def line(tp_count):
    sp = lax.axis_index("sp")
    tp = lax.axis_index("tp")
    core = lax.rem(tp, 2)
    z = lax.div(tp, 2)
    depth = tp_count // 2
    partner = (sp, tp + 1 - 2 * core)
    return sp, core, z, depth, partner, (sp, tp + 2), (sp, tp - 2), z < depth - 1, z > 0


def moe_kernel(
    sp_count,
    tp_count,
    heads_ref,
    residual_ref,
    norm_gain_ref,
    extra_ref,
    rank_ref,
    gate_ref,
    up_ref,
    down_ref,
    out_ref,
    own,
    token_rows,
    pick,
    back_pick,
    held,
    picked,
    rows,
    gate,
    up,
    down,
    result,
    swapped,
    summed,
    back,
    mixed,
    stage,
    up_in,
    down_in,
    usend,
    dsend,
    recv,
    ssend,
    srecv,
    fsend,
    frecv,
    wsend,
    wrecv,
    rsend,
    rrecv,
    zsend,
    urecv,
    drecv,
    wsem,
):
    me, core, z, depth, partner, above, below, has_above, has_below = line(tp_count)
    tp = lax.axis_index("tp")
    experts = gate_ref.shape[0]
    model = gate_ref.shape[1]
    tokens, wide = own.shape
    slots = rows.shape[3]
    low = own.dtype
    gather_parts = (slice(0, wide // 256 * 128), slice(wide // 256 * 128, wide))
    parts = (slice(0, model // 256 * 128), slice(model // 256 * 128, model))
    others = [lax.rem(me + k, sp_count) for k in reversed(range(1, sp_count))]
    loads = [
        pltpu.make_async_copy(source, target, wsem.at[i])
        for i, (source, target) in enumerate(((gate_ref, gate), (up_ref, up), (down_ref, down)))
    ]
    for load in loads:
        load.start()
    total = residual_ref[...].astype(jnp.float32) + heads_ref[...]
    token_rows[...] = total
    own[:, :model] = rms_scale(total, norm_gain_ref[...]).astype(low)
    own[:, model:] = extra_ref[...]
    greet_some(
        [(True, partner), (has_above, above), (has_below, below)]
        + [(True, (other, tp)) for other in others]
    )

    def move(place, sems, part, target, source=None):
        source = held.at[place] if source is None else source
        return remote(
            source.at[:, gather_parts[part]],
            held.at[place, :, gather_parts[part]],
            sems.at[place, part],
            recv.at[place, part],
            target,
        )

    for part in range(2):

        @pl.when(has_above)
        def _():
            move(z, usend, part, above, own).start()

        @pl.when(has_below)
        def _():
            move(z, dsend, part, below, own).start()

    held[z] = own[...]
    slot = lax.broadcasted_iota(jnp.int32, (slots, tokens), 0)
    for place in range(depth):
        chosen = [
            jnp.where(rank_ref[place, source : source + 1] == slot, 1.0, 0.0)
            for source in range(sp_count)
        ]
        chosen = jnp.concatenate(chosen, axis=0)
        pick[place] = chosen.astype(low)
        back_pick[place] = chosen.T.astype(low)

    def send_to(source, target, sends, recvs, place, part, mark, arrive, device):
        return remote(
            source, target, sends.at[place, mark, part], recvs.at[place, arrive, part], device
        )

    def spread(place, part, other, arrive=None):
        arrive = me if arrive is None else arrive
        span = gather_parts[part]
        return send_to(
            picked.at[place, other, :, span],
            rows.at[place, core, arrive, :, span],
            ssend,
            srecv,
            place,
            part,
            other,
            arrive,
            (other, tp),
        )

    def share(place, part, source, own_rows=False):
        span = gather_parts[part]
        target = rows.at[place, core, source, :, span]
        start = picked.at[place, source, :, span] if own_rows else target
        return send_to(start, target, fsend, frecv, place, part, source, source, partner)

    def shared(place, part, source):
        target = rows.at[place, 1 - core, source, :, gather_parts[part]]
        return send_to(target, target, fsend, frecv, place, part, source, source, partner)

    def swap(place, part):
        return remote(
            result.at[place, 1 - core, :, :, parts[part]],
            swapped.at[place, :, :, parts[part]],
            wsend.at[place, part],
            wrecv.at[place, part],
            partner,
        )

    def give(place, part, other, arrive=None):
        arrive = me if arrive is None else arrive
        span = parts[part]
        return send_to(
            summed.at[place, other, :, span],
            back.at[place, arrive, :, span],
            rsend,
            rrecv,
            place,
            part,
            other,
            arrive,
            (other, tp),
        )

    def pass_on(place, part, arrivals, sems, target):
        return remote(
            stage.at[place, :, parts[part]],
            arrivals.at[place, :, parts[part]],
            zsend.at[place, part],
            sems.at[place, part],
            target,
        )

    def rise(place, part):
        return pass_on(place, part, up_in, urecv, above)

    def fall(place, part):
        return pass_on(place, part, down_in, drecv, below)

    def take(k, part):
        lower, upper = z - k, z + k

        @pl.when((k > 0) & (lower >= 0))
        def _():
            move(lower, usend, part, below).wait_recv()

            @pl.when(has_above)
            def _():
                move(lower, usend, part, above).start()

        @pl.when((k > 0) & (upper < depth))
        def _():
            move(upper, dsend, part, above).wait_recv()

            @pl.when(has_below)
            def _():
                move(upper, dsend, part, below).start()

    def choose(place, part):
        span = gather_parts[part]
        chosen = jnp.dot(pick[place], held[place, :, span], preferred_element_type=jnp.float32)
        picked[place, :, :, span] = chosen.astype(low).reshape(
            sp_count, slots, span.stop - span.start
        )
        for other in others:
            spread(place, part, other).start()
        share(place, part, me, True).start()
        rows[place, core, me, :, span] = picked[place, me, :, span]

    def relay(place, part):
        for other in others:
            spread(place, part, other, other).wait_recv()
            share(place, part, other).start()

    def compute(place):
        for part in range(2):
            for source in range(sp_count):
                shared(place, part, source).wait_recv()
        x = rows[place].reshape(2 * sp_count * slots, wide)
        inputs = x[:, :model]
        tail = x[:, model:].astype(jnp.float32)
        lane = lax.broadcasted_iota(jnp.int32, tail.shape, 1)
        hidden = []
        for e in range(experts):
            index = me * experts + e
            here = (lane == index) | (lane == index + experts * sp_count)
            scale = jnp.sum(jnp.where(here, tail, 0.0), axis=1, keepdims=True)
            gate_out = jnp.dot(inputs, gate[e], preferred_element_type=jnp.float32)
            up_out = jnp.dot(inputs, up[e], preferred_element_type=jnp.float32)
            hidden.append((jax.nn.silu(gate_out) * up_out * scale).astype(low))
        for part in range(2):
            span = parts[part]
            total = jnp.dot(hidden[0], down[0, :, span], preferred_element_type=jnp.float32)
            for e in range(1, experts):
                total += jnp.dot(hidden[e], down[e, :, span], preferred_element_type=jnp.float32)
            result[place, :, :, :, span] = total.astype(low).reshape(
                2, sp_count, slots, span.stop - span.start
            )
            swap(place, part).start()

    def settle(place, part):
        span = parts[part]
        swap(place, part).wait_recv()
        kept = result[place, core, :, :, span].astype(jnp.float32)
        both = kept + swapped[place, :, :, span].astype(jnp.float32)
        summed[place, :, :, span] = both.astype(low)
        for other in others:
            give(place, part, other).start()
        back[place, me, :, span] = summed[place, me, :, span]

    def combine(place, part):
        span = parts[part]
        for other in others:
            give(place, part, other, other).wait_recv()
        mixed[place, :, span] = jnp.dot(
            back_pick[place],
            back[place, :, :, span].reshape(sp_count * slots, span.stop - span.start),
            preferred_element_type=jnp.float32,
        )

        @pl.when((place > z) & (z == 0))
        def _():
            stage[place, :, span] = mixed[place, :, span].astype(low)
            rise(place, part).start()

        @pl.when((place < z) & (z == depth - 1))
        def _():
            stage[place, :, span] = mixed[place, :, span].astype(low)
            fall(place, part).start()

    def at(k, action):
        def one(side, unused):
            place = z + (1 - 2 * side) * k

            @pl.when((place >= 0) & (place < depth) & ((k > 0) | (side == 0)) & (k >= 0))
            def _():
                action(place)

            return unused

        lax.fori_loop(0, 2, one, 0)

    def step(t, unused):
        @pl.when(t < depth)
        def _():
            for part in range(2):
                take(t, part)
                at(t, lambda place: choose(place, part))

        @pl.when(t == 1)
        def _():
            for load in loads:
                load.wait()

        for action, late in ((relay, 1), (settle, 2), (combine, 3)):
            for part in range(2):
                at(t - late, lambda place: action(place, part))
        at(t - 1, compute)
        return unused

    lax.fori_loop(0, depth + 3, step, 0)

    def hop(key, unused):
        high = key - z
        deep = 2 * depth - 2 - key - z
        for part in range(2):
            span = parts[part]

            @pl.when((high > z) & (high < depth) & has_below)
            def _():
                rise(high, part).wait_recv()
                stage[high, :, span] = (
                    mixed[high, :, span] + up_in[high, :, span].astype(jnp.float32)
                ).astype(low)
                rise(high, part).start()

            @pl.when((deep >= 0) & (deep < z) & has_above)
            def _():
                fall(deep, part).wait_recv()
                stage[deep, :, span] = (
                    mixed[deep, :, span] + down_in[deep, :, span].astype(jnp.float32)
                ).astype(low)
                fall(deep, part).start()

        return unused

    lax.fori_loop(1, 2 * depth - 2, hop, 0)
    for part in range(2):
        span = parts[part]
        token_rows[:, span] += mixed[z, :, span]

        @pl.when(has_below)
        def _():
            rise(z, part).wait_recv()
            token_rows[:, span] += up_in[z, :, span].astype(jnp.float32)

        @pl.when(has_above)
        def _():
            fall(z, part).wait_recv()
            token_rows[:, span] += down_in[z, :, span].astype(jnp.float32)

        out_ref[:, span] = token_rows[:, span].astype(low)

    def finish(place, unused):
        for part in range(2):

            @pl.when(has_above & (place <= z))
            def _():
                move(place, usend, part, above).wait_send()

            @pl.when(has_below & (place >= z))
            def _():
                move(place, dsend, part, below).wait_send()

            @pl.when(place > z)
            def _():
                rise(place, part).wait_send()

            @pl.when(place < z)
            def _():
                fall(place, part).wait_send()

            for other in others:
                spread(place, part, other).wait_send()
                share(place, part, other).wait_send()
                give(place, part, other).wait_send()
            share(place, part, me, True).wait_send()
            swap(place, part).wait_send()
        return unused

    lax.fori_loop(0, depth, finish, 0)


def moe(
    heads,
    residual,
    norm_gain,
    extra,
    rank,
    slots,
    gate_weight,
    up_weight,
    down_weight,
    sp_count,
    tp_count,
    identity,
):
    dma = pltpu.SemaphoreType.DMA
    depth = tp_count // 2
    tokens, model = residual.shape
    wide = model + extra.shape[1]
    low = residual.dtype
    anywhere = pl.BlockSpec(memory_space=pl.ANY)
    each = dma((depth, sp_count, 2))
    two = dma((depth, 2))
    block = pltpu.VMEM((depth, tokens, model), low)
    group = pltpu.VMEM((depth, sp_count, slots, model), low)
    return pl.pallas_call(
        functools.partial(moe_kernel, sp_count, tp_count),
        out_shape=jax.ShapeDtypeStruct((tokens, model), low),
        in_specs=[VM, VM, VM, VM, VM, anywhere, anywhere, anywhere],
        out_specs=VM,
        scratch_shapes=[
            pltpu.VMEM((tokens, wide), low),
            pltpu.VMEM((tokens, model), jnp.float32),
            pltpu.VMEM((depth, sp_count * slots, tokens), low),
            pltpu.VMEM((depth, tokens, sp_count * slots), low),
            pltpu.VMEM((depth, tokens, wide), low),
            pltpu.VMEM((depth, sp_count, slots, wide), low),
            pltpu.VMEM((depth, 2, sp_count, slots, wide), low),
            pltpu.VMEM(gate_weight.shape, gate_weight.dtype),
            pltpu.VMEM(up_weight.shape, up_weight.dtype),
            pltpu.VMEM(down_weight.shape, down_weight.dtype),
            pltpu.VMEM((depth, 2, sp_count, slots, model), low),
            group,
            group,
            group,
            pltpu.VMEM((depth, tokens, model), jnp.float32),
            block,
            block,
            block,
            two,
            two,
            two,
            each,
            each,
            each,
            each,
            two,
            two,
            each,
            each,
            two,
            two,
            two,
            dma((3,)),
        ],
        compiler_params=pltpu.CompilerParams(
            collective_id=identity, has_side_effects=True, vmem_limit_bytes=60 * 1024 * 1024
        ),
    )(heads, residual, norm_gain[None, :], extra, rank, gate_weight, up_weight, down_weight)


NT = (((1,), (1,)), ((), ()))


def attend_kernel(
    rope_width,
    sp_count,
    tp_count,
    latent_ref,
    gain_ref,
    key_rope_ref,
    q_ref,
    q_rope_ref,
    cos_ref,
    sin_ref,
    wk_ref,
    wv_ref,
    wo_ref,
    out_ref,
    latent,
    queries,
    wk_raw,
    wv_raw,
    wo,
    own,
    held,
    qx,
    wk,
    wvt,
    kx,
    vt,
    tops,
    sums,
    acc,
    attention,
    partial,
    partner_in,
    stage,
    up_in,
    down_in,
    wsem,
    send,
    recv,
    fsend,
    psend,
    precv,
    zsend,
    urecv,
    drecv,
):
    me, core, z, depth, partner, above, below, has_above, has_below = line(tp_count)
    tp = lax.axis_index("tp")
    tokens, width = latent.shape
    pairs, pair_width = queries.shape[1:]
    half = tokens // 2
    low = own.dtype
    loads = [
        pltpu.make_async_copy(source, target, wsem.at[i])
        for i, (source, target) in enumerate(
            (
                (latent_ref, latent),
                (q_ref, queries),
                (wk_ref, wk_raw),
                (wv_ref, wv_raw),
                (wo_ref, wo),
            )
        )
    ]
    for load in loads:
        load.start()
    mine = pl.ds(pl.multiple_of(core * half, half), half)
    other = pl.ds(pl.multiple_of((1 - core) * half, half), half)

    def outgoing(to):
        return remote(own.at[mine], held.at[me, mine], send.at[to], recv.at[me, core], (to, tp))

    def incoming(source):
        return remote(
            own.at[mine], held.at[source, mine], send.at[source], recv.at[source, core], partner
        )

    def forward(source):
        return remote(
            held.at[source, mine],
            held.at[source, mine],
            fsend.at[source],
            recv.at[source, core],
            partner,
        )

    def forwarded(source):
        return remote(
            held.at[source, other],
            held.at[source, other],
            fsend.at[source],
            recv.at[source, 1 - core],
            partner,
        )

    turn = rope_width // 2
    cosine, sine = cos_ref[...], sin_ref[...]

    def rotate(upper, lower):
        return upper * cosine - lower * sine, lower * cosine + upper * sine

    raw = key_rope_ref[...].astype(jnp.float32)
    rotated = list(rotate(raw[:turn], raw[turn:]))
    own[:, width:] = jnp.concatenate(rotated * (128 // rope_width), axis=0).T.astype(low)
    loads[0].wait()
    values = latent[...].astype(jnp.float32)
    inverse = lax.rsqrt(jnp.mean(values * values, axis=-1, keepdims=True) + epsilon)
    own[:, :width] = (values * inverse * gain_ref[...]).astype(low)

    greet_some(
        [(True, partner), (has_above, above), (has_below, below)]
        + [(True, (lax.rem(me + k, sp_count), tp)) for k in range(1, sp_count)]
    )
    for to in reversed(range(sp_count)):

        @pl.when(to > me)
        def _():
            outgoing(to).start()

    def merge(one, two):
        lane = lax.broadcasted_iota(jnp.int32, one.shape, 1)
        return jnp.where(lane < DK_A, one, two)

    for load in loads[1:]:
        load.wait()
    gap = jnp.zeros((DK_A - rope_width, tokens), jnp.float32)
    for pair in range(pairs):
        rope = q_rope_ref[pair].astype(jnp.float32)
        first = list(rotate(rope[:turn], rope[turn:rope_width]))
        second = list(rotate(rope[rope_width : rope_width + turn], rope[rope_width + turn :]))
        turned = jnp.concatenate(second + [gap] + first + [gap], axis=0).T.astype(low)
        qx[pair, :, 128:] = queries[:, pair, :]
        query = qx[pair, :, 128:256]
        qx[pair, :, :128] = merge(query, turned)
        qx[pair, :, 128:256] = merge(turned, query)
        wk[pair] = wk_raw[:, pair, :]
        wvt[pair] = wv_raw[:, pair, :].T
    scales = [
        size ** (-0.5) * 1.4426950408889634
        for size in (DK_A + rope_width, pair_width - DK_A + rope_width)
    ]
    splits = ((slice(0, 128), slice(0, DV_A)), (slice(128, None), slice(DV_A, pair_width)))

    def block(index, first):
        source = own if first else held.at[index]
        compressed = source[:, :width]
        rope = source[:, width:]
        for pair in range(pairs):
            rows = jnp.dot(compressed, wk[pair], preferred_element_type=jnp.float32).astype(low)
            kx[pair, :, :128] = merge(rows[:, :128], rope)
            kx[pair, :, 128:256] = merge(rope, rows[:, :128])
            kx[pair, :, 256:] = rows[:, 128:]
            vt[pair] = lax.dot_general(
                wvt[pair], compressed, NT, preferred_element_type=jnp.float32
            ).astype(low)
        for pair in range(pairs):
            for group, (span, part) in enumerate(splits):
                head = pair * 2 + group
                scores = lax.dot_general(
                    kx[pair, :, span], qx[pair, :, span], NT, preferred_element_type=jnp.float32
                )
                if first:
                    row = lax.broadcasted_iota(jnp.int32, (tokens, tokens), 0)
                    column = lax.broadcasted_iota(jnp.int32, (tokens, tokens), 1)
                    scores = jnp.where(row <= column, scores, floor_score)
                    top = jnp.max(scores, axis=0, keepdims=True)
                else:
                    old = tops[head]
                    top = jnp.maximum(old, jnp.max(scores, axis=0, keepdims=True))
                    factor = jnp.exp2((old - top) * scales[group])
                weights = jnp.exp2((scores - top) * scales[group])
                total = jnp.sum(weights, axis=0, keepdims=True)
                update = jnp.dot(
                    vt[pair, part], weights.astype(low), preferred_element_type=jnp.float32
                )
                tops[head] = top
                if first:
                    sums[head] = total
                    acc[pair, part] = update
                else:
                    sums[head] = sums[head] * factor + total
                    acc[pair, part] = acc[pair, part] * factor + update

    block(me, True)

    def step(i, unused):
        index = me - 1 - i
        incoming(index).wait_recv()
        forward(index).start()
        forwarded(index).wait_recv()
        block(index, False)
        return unused

    lax.fori_loop(0, me, step, 0)
    for pair in range(pairs):
        for group, (span, part) in enumerate(splits):
            acc[pair, part] = acc[pair, part] / sums[pair * 2 + group]
        attention[:, pair * pair_width : (pair + 1) * pair_width] = acc[pair].T.astype(low)

    row_count, model = out_ref.shape
    middle = model // 256 * 128
    parts = (slice(0, middle), slice(middle, model))

    def swap(place, part):
        return remote(
            partial.at[place * 2 + 1 - core, :, parts[part]],
            partner_in.at[place, :, parts[part]],
            psend.at[place, part],
            precv.at[place, part],
            partner,
        )

    def pass_on(place, part, arrivals, sems, target):
        return remote(
            stage.at[place, :, parts[part]],
            arrivals.at[place, :, parts[part]],
            zsend.at[place, part],
            sems.at[place, part],
            target,
        )

    def up(place, part):
        return pass_on(place, part, up_in, urecv, above)

    def down(place, part):
        return pass_on(place, part, down_in, drecv, below)

    def pair_sum(place, part):
        swap(place, part).wait_recv()
        kept = partial[place * 2 + core, :, parts[part]].astype(jnp.float32)
        return kept + partner_in[place, :, parts[part]].astype(jnp.float32)

    def project(n, unused):
        turnabout = lax.rem(n, 2)
        place = turnabout * (n // 2) + (1 - turnabout) * (depth - 1 - n // 2)
        rows = pl.ds(pl.multiple_of(place * 2 * row_count, 2 * row_count), 2 * row_count)
        inputs = attention[rows]
        for part in range(2):
            mixed = jnp.dot(inputs, wo[:, parts[part]], preferred_element_type=jnp.float32)
            mixed = mixed.astype(low).reshape(2, row_count, mixed.shape[1])
            partial[pl.ds(place * 2, 2), :, parts[part]] = mixed
            swap(place, part).start()
        return unused

    lax.fori_loop(0, depth, project, 0)

    for j in range(depth - 1):
        high, deep = depth - 1 + z - j, j + z + 1 - depth
        for part in range(2):
            span = parts[part]

            @pl.when(z <= j)
            def _():
                stage[high, :, span] = pair_sum(high, part).astype(low)

                @pl.when(has_below)
                def _():
                    up(high, part).wait_recv()
                    stage[high, :, span] = (
                        stage[high, :, span].astype(jnp.float32)
                        + up_in[high, :, span].astype(jnp.float32)
                    ).astype(low)

                up(high, part).start()

            @pl.when(deep >= 0)
            def _():
                stage[deep, :, span] = pair_sum(deep, part).astype(low)

                @pl.when(has_above)
                def _():
                    down(deep, part).wait_recv()
                    stage[deep, :, span] = (
                        stage[deep, :, span].astype(jnp.float32)
                        + down_in[deep, :, span].astype(jnp.float32)
                    ).astype(low)

                down(deep, part).start()

    for part in range(2):
        span = parts[part]
        out_ref[:, span] = pair_sum(z, part)

        @pl.when(has_below)
        def _():
            up(z, part).wait_recv()
            out_ref[:, span] += up_in[z, :, span].astype(jnp.float32)

        @pl.when(has_above)
        def _():
            down(z, part).wait_recv()
            out_ref[:, span] += down_in[z, :, span].astype(jnp.float32)

    for place in range(sp_count):

        @pl.when(place < me)
        def _():
            forward(place).wait_send()

        @pl.when(place > me)
        def _():
            outgoing(place).wait_send()

    for place in range(depth):
        for part in range(2):
            swap(place, part).wait_send()

            @pl.when(place > z)
            def _():
                up(place, part).wait_send()

            @pl.when(place < z)
            def _():
                down(place, part).wait_send()


def attend(
    latent,
    latent_gain,
    key_rope,
    queries,
    query_rope,
    cosine,
    sine,
    key_weight,
    value_weight,
    out_weight,
    sp_count,
    tp_count,
    identity,
):
    tokens, latent_width = latent.shape
    pairs, pair_width = queries.shape[1:]
    rope_width = key_rope.shape[1]
    model = out_weight.shape[1]
    low = latent.dtype
    row_count = tokens // tp_count
    depth = tp_count // 2
    dma = pltpu.SemaphoreType.DMA
    vmem = pltpu.VMEM
    f32 = jnp.float32
    padded = pair_width + 128
    anywhere = pl.BlockSpec(memory_space=pl.ANY)
    block = vmem((depth, row_count, model), low)
    return pl.pallas_call(
        functools.partial(attend_kernel, rope_width, sp_count, tp_count),
        out_shape=jax.ShapeDtypeStruct((row_count, model), f32),
        in_specs=[anywhere, VM, VM, anywhere, VM, VM, VM, anywhere, anywhere, anywhere],
        out_specs=VM,
        scratch_shapes=[
            vmem(latent.shape, low),
            vmem(queries.shape, low),
            vmem(key_weight.shape, low),
            vmem(value_weight.shape, low),
            vmem(out_weight.shape, low),
            vmem((tokens, latent_width + 128), low),
            vmem((sp_count, tokens, latent_width + 128), low),
            vmem((pairs, tokens, padded), low),
            vmem((pairs, latent_width, pair_width), low),
            vmem((pairs, pair_width, latent_width), low),
            vmem((pairs, tokens, padded), low),
            vmem((pairs, pair_width, tokens), low),
            vmem((2 * pairs, 1, tokens), f32),
            vmem((2 * pairs, 1, tokens), f32),
            vmem((pairs, pair_width, tokens), f32),
            vmem((tokens, pairs * pair_width), low),
            vmem((tp_count, row_count, model), low),
            block,
            block,
            block,
            block,
            dma((5,)),
            dma((sp_count,)),
            dma((sp_count, 2)),
            dma((sp_count,)),
            dma((depth, 2)),
            dma((depth, 2)),
            dma((depth, 2)),
            dma((depth, 2)),
            dma((depth, 2)),
        ],
        compiler_params=pltpu.CompilerParams(
            collective_id=identity, has_side_effects=True, vmem_limit_bytes=60 * 1024 * 1024
        ),
    )(
        latent,
        latent_gain[None, :],
        key_rope.T,
        queries,
        query_rope.transpose(1, 2, 0),
        cosine,
        sine,
        key_weight,
        value_weight,
        out_weight,
    )


def local(
    residual,
    queries,
    query_rope,
    latent,
    key_rope,
    latent_gain,
    key_weight,
    value_weight,
    out_weight,
    norm_gain,
    routes,
    group_gate,
    expert_share,
    gate_weight,
    up_weight,
    down_weight,
):
    tokens = queries.shape[0]
    pair_dev = queries.shape[1]
    sp_count = lax.axis_size("sp")
    tp_count = lax.axis_size("tp")
    row_count = tokens // tp_count
    rope_width = key_rope.shape[1]
    low = jnp.bfloat16

    first_place = lax.axis_index("sp") * tokens
    places = (first_place + jnp.arange(tokens, dtype=jnp.int32)).astype(jnp.float32)
    cosine, sine = angle_tables(places, rope_width)
    head_total = attend(
        latent,
        latent_gain,
        key_rope,
        queries,
        query_rope,
        cosine,
        sine,
        key_weight,
        value_weight,
        out_weight.reshape(-1, residual.shape[1]),
        sp_count,
        tp_count,
        0,
    )
    routes, group_gate, expert_share, head_total = lax.optimization_barrier(
        (routes, group_gate, expert_share, head_total)
    )
    experts_dev = gate_weight.shape[0]
    experts_all = experts_dev * sp_count
    top_count = routes.shape[1]
    depth = tp_count // 2
    capacity = max(2, 3 * row_count * top_count // (2 * experts_all))
    slots = experts_dev * capacity
    if experts_all // GROUPS == experts_dev == top_count:
        slots = capacity
    slots = -(-slots // 8) * 8
    tp = lax.axis_index("tp")
    own = lax.dynamic_slice_in_dim(routes, tp * row_count, row_count, 0)
    route_weight = group_gate[:, None] * expert_share / jnp.sum(expert_share, axis=1, keepdims=True)
    expert_ids = jnp.arange(experts_all, dtype=jnp.int32)
    named = own[:, :, None] == expert_ids[None, None, :]
    table = jnp.sum(jnp.where(named, route_weight[:, :, None], 0.0), axis=1)
    weight_high = table.astype(low)
    weight_low = (table - weight_high.astype(jnp.float32)).astype(low)
    extra = jnp.concatenate([weight_high, weight_low], axis=1)
    extra = jnp.pad(extra, ((0, 0), (0, 128 - extra.shape[1])))

    column = lax.dynamic_index_in_dim(
        routes.reshape(depth, 2, row_count, top_count), lax.rem(tp, 2), 1, keepdims=False
    )
    goal = column // experts_dev
    member = jnp.any(goal[:, :, :, None] == jnp.arange(sp_count, dtype=jnp.int32), axis=2)
    row = jnp.arange(row_count, dtype=jnp.int32)
    earlier = (row[:, None] > row[None, :]).astype(low)
    member = member.astype(low)
    rank = jnp.einsum("rq,zqs->zsr", earlier, member, preferred_element_type=jnp.float32)
    rank = jnp.where(jnp.swapaxes(member, 1, 2) > 0, rank.astype(jnp.int32), -1)
    return moe(
        head_total,
        residual,
        norm_gain,
        extra,
        rank,
        slots,
        gate_weight,
        up_weight,
        down_weight,
        sp_count,
        tp_count,
        3,
    )


def solution(mesh):
    return jax.shard_map(
        local,
        mesh=mesh,
        in_specs=(
            P(("sp", "tp"), None),
            P("sp", "tp", None),
            P("sp", "tp", None),
            P("sp", None),
            P("sp", None),
            P(),
            P(None, "tp", None),
            P(None, "tp", None),
            P("tp", None, None),
            P(),
            P("sp", None),
            P(("sp", "tp")),
            P(("sp", "tp"), None),
            P("sp", None, "tp"),
            P("sp", None, "tp"),
            P("sp", "tp", None),
        ),
        out_specs=P(("sp", "tp"), None),
        check_vma=False,
    )
```

time: 121 us -> 108 us (0.89)
  other arithmetic: 8.82 us -> 0.86 us
  local copies, waits for them, and re-layouts: 6.36 us -> 2.51 us
    convert_element_type x6 -> x0, other arithmetic: 4.38 us -> none  [the longest x1 1.72 us: local(): return (mixed_rows + expert_mix).astype(low)]
    unnamed x11 -> x7, local copies, waits for them, and re-layouts: 3.33 us -> 1.63 us
    reduce_sum x2 -> x0, other arithmetic: 1.32 us -> none  [rms_scale(): jnp.mean(values * values, axis=-1, keepdims=True) + epsilon]
    pallas_call x2 -> x1, Pallas kernels: 32.4 us -> 31.6 us  [attend(): pl.pallas_call(functools.partial(attend_kernel, rope_width, sp_count, tp_...]
where the time goes in v2:
time: 108 us
  Pallas kernels  104 us (96%)
  local copies, waits for them, and re-layouts  2.51 us (2%)
    pallas_call x1, Pallas kernels, moe(): pl.pallas_call(functools.partial(moe_kernel, sp_count, tp_count), out_sha...  72.3 us
    pallas_call x1, Pallas kernels, attend(): pl.pallas_call(functools.partial(attend_kernel, rope_width, sp_count, tp_...  31.6 us

profile of v2, /device:TPU:0, one launch (start us, length us, event | category | flops | bytes accessed | tf_op | source)
XLA Modules:
  0.0 108.1 jit_solution(14654270897097138990)
XLA Ops:
  0.0 0.0 copy-start.1
  0.0 0.0 copy-start.2
  0.0 0.0 copy-start
  0.0 0.8 multiply_sine_fusion
  0.8 31.6 %shard_map.154.heads_ref = f32[48,2048]{1,0:T(8,128)} custom-call(bf16[384,512]{1,0:T(8,128)(2,1)} %latent_ref.1, f32[1,512]{1,0:T(1,128)} %bitcast.21, bf16[32,384]{1,0:T(8,128)(2,1)} %bitcast.18, bf16[384,2,256]{2,1,0:T(2,128)(2,1)} %q_ref.1, bf16[2,64,384]{2,1,0:T(8,128)(2,1)} %bitcast.17, f32[16,384]{1,0:T(8,128)} %get-tuple-element.16.cos_ref, ...), custom_call_target="tpu_custom_call" | custom-call | tf_op jit(solution)/shard_map/pallas_call | solution.py:850
  32.4 0.0 copy-done
  32.4 0.1 constant_dynamic-slice_fusion.1
  32.5 0.0 copy-done.1
  32.5 0.0 copy-done.2
  32.6 0.1 copy.37
  32.7 0.6 pad.4.extra_ref
  33.3 0.1 reshape.52
  33.4 0.7 fusion.rank_ref
  34.2 72.3 %shard_map.155 = bf16[48,2048]{1,0:T(8,128)(2,1)} custom-call(f32[48,2048]{1,0:T(8,128)} %shard_map.154.heads_ref, bf16[48,2048]{1,0:T(8,128)(2,1)} %residual_ref.1, f32[1,2048]{1,0:T(1,128)} %bitcast.20, bf16[48,128]{1,0:T(8,128)(2,1)} %pad.4.extra_ref, s32[4,4,48]{2,1,0:T(4,128)} %fusion.rank_ref, bf16[2,2048,512]{2,1,0:T(8,128)(2,1)} %gate_ref.1, ...), custom_call_target="tpu_custom_call" | custom-call | tf_op jit(solution)/shard_map/pallas_call | solution.py:457
  106.5 1.6 %copy.42 = bf16[48,2048]{1,0:T(8,128)(2,1)} copy(bf16[48,2048]{1,0:T(8,128)(2,1)} %shard_map.155) | data formatting | bytes 393216
  (11 shorter events, 0.1 us)
Async XLA Ops:
  0.0 32.5 %copy-start.1 = (f32[48,2]{0,1:T(2,128)S(1)}, f32[48,2]{0,1:T(2,128)}, u32[]{:S(2)}) copy-start(f32[48,2]{0,1:T(2,128)} %param.28) | copy-start | bytes 1156
  0.0 32.5 %copy-start.2 = (f32[48]{0:T(128)S(1)}, f32[48]{0:T(128)}, u32[]{:S(2)}) copy-start(f32[48]{0:T(128)} %param.27) | copy-start | bytes 580
  0.0 32.4 %copy-start = (s32[384,2]{0,1:T(2,128)S(1)}, s32[384,2]{0,1:T(2,128)}, u32[]{:S(2)}) copy-start(s32[384,2]{0,1:T(2,128)} %param.26) | copy-start | bytes 9220

commit v3 on v2

--- a/solution.py
+++ b/solution.py
@@ -52,7 +52,7 @@
             pl.semaphore_signal(barrier, inc=1, device_id=target, device_id_type=MESH)
 
         count = count + jnp.where(here, 1, 0)
-    pl.semaphore_wait(barrier, count)
+    return lambda: pl.semaphore_wait(barrier, count)
 
 
 def line(tp_count):
@@ -68,6 +68,7 @@
 def moe_kernel(
     sp_count,
     tp_count,
+    spare,
     heads_ref,
     residual_ref,
     norm_gain_ref,
@@ -79,8 +80,6 @@
     out_ref,
     own,
     token_rows,
-    pick,
-    back_pick,
     held,
     picked,
     rows,
@@ -88,7 +87,9 @@
     up,
     down,
     result,
+    result_spare,
     swapped,
+    swapped_spare,
     summed,
     back,
     mixed,
@@ -104,6 +105,8 @@
     frecv,
     wsend,
     wrecv,
+    vsend,
+    vrecv,
     rsend,
     rrecv,
     zsend,
@@ -118,29 +121,79 @@
     tokens, wide = own.shape
     slots = rows.shape[3]
     low = own.dtype
-    gather_parts = (slice(0, wide // 256 * 128), slice(wide // 256 * 128, wide))
-    parts = (slice(0, model // 256 * 128), slice(model // 256 * 128, model))
+    middle = model // 2
+    segment = middle * spare // slots
+    sent = middle + segment
+    line_parts = (slice(0, middle), slice(middle, wide))
+    parts = (slice(0, middle), slice(middle, model))
+    gather_parts = (slice(0, sent), slice(sent, rows.shape[4]))
+    return_parts = (slice(0, sent), slice(sent, 2 * sent))
+
+    def fold_matrix(k, count, flat):
+        full, few = count * slots, count * spare
+        shape = (full, few) if flat else (few, full)
+        row = lax.broadcasted_iota(jnp.int32, shape, 0 if flat else 1)
+        column = lax.broadcasted_iota(jnp.int32, shape, 1 if flat else 0)
+        place = row & (slots - 1)
+        low_bits = spare.bit_length() - 1
+        owner = (row >> (slots.bit_length() - 1)) << low_bits
+        here = ((place >> low_bits) == k) & (column == owner + (row & (spare - 1)))
+        return jnp.where(here, 1.0, 0.0).astype(low)
+
+    def fold(extra_rows):
+        count = extra_rows.shape[0] // spare
+        total = None
+        for k in range(slots // spare):
+            piece = extra_rows[:, k * segment : (k + 1) * segment]
+            matrix = fold_matrix(k, count, True)
+            term = jnp.dot(matrix, piece, preferred_element_type=jnp.float32)
+            total = term if k == 0 else total + term
+        return total.astype(low)
+
+    def unfold(folded):
+        count = folded.shape[0] // slots
+        pieces = [
+            jnp.dot(fold_matrix(k, count, False), folded, preferred_element_type=jnp.float32)
+            for k in range(slots // spare)
+        ]
+        return jnp.concatenate(pieces, axis=1).astype(low)
+
+    def one_hot(place, start, height, limit):
+        row = lax.broadcasted_iota(jnp.int32, (height, tokens), 0)
+        wanted = jnp.where(row < limit, row + start, -2)
+        pieces = [
+            jnp.where(rank_ref[place, source : source + 1] == wanted, 1.0, 0.0)
+            for source in range(sp_count)
+        ]
+        return jnp.concatenate(pieces, axis=0)
+
+    def spare_hot(place):
+        full = one_hot(place, slots, slots, spare)
+        matrix = fold_matrix(0, sp_count, False)
+        return jnp.dot(matrix, full.astype(low), preferred_element_type=jnp.float32)
+
     others = [lax.rem(me + k, sp_count) for k in reversed(range(1, sp_count))]
     loads = [
         pltpu.make_async_copy(source, target, wsem.at[i])
         for i, (source, target) in enumerate(((gate_ref, gate), (up_ref, up), (down_ref, down)))
     ]
+    met = greet_some(
+        [(True, partner), (has_above, above), (has_below, below)]
+        + [(True, (other, tp)) for other in others]
+    )
     for load in loads:
         load.start()
     total = residual_ref[...].astype(jnp.float32) + heads_ref[...]
     token_rows[...] = total
     own[:, :model] = rms_scale(total, norm_gain_ref[...]).astype(low)
     own[:, model:] = extra_ref[...]
-    greet_some(
-        [(True, partner), (has_above, above), (has_below, below)]
-        + [(True, (other, tp)) for other in others]
-    )
+    met()
 
     def move(place, sems, part, target, source=None):
         source = held.at[place] if source is None else source
         return remote(
-            source.at[:, gather_parts[part]],
-            held.at[place, :, gather_parts[part]],
+            source.at[:, line_parts[part]],
+            held.at[place, :, line_parts[part]],
             sems.at[place, part],
             recv.at[place, part],
             target,
@@ -157,16 +210,6 @@
             move(z, dsend, part, below, own).start()
 
     held[z] = own[...]
-    slot = lax.broadcasted_iota(jnp.int32, (slots, tokens), 0)
-    for place in range(depth):
-        chosen = [
-            jnp.where(rank_ref[place, source : source + 1] == slot, 1.0, 0.0)
-            for source in range(sp_count)
-        ]
-        chosen = jnp.concatenate(chosen, axis=0)
-        pick[place] = chosen.astype(low)
-        back_pick[place] = chosen.T.astype(low)
-
     def send_to(source, target, sends, recvs, place, part, mark, arrive, device):
         return remote(
             source, target, sends.at[place, mark, part], recvs.at[place, arrive, part], device
@@ -206,9 +249,18 @@
             partner,
         )
 
+    def swap_spare(place, part):
+        return remote(
+            result_spare.at[place, 1 - core, :, parts[part]],
+            swapped_spare.at[place, :, parts[part]],
+            vsend.at[place, part],
+            vrecv.at[place, part],
+            partner,
+        )
+
     def give(place, part, other, arrive=None):
         arrive = me if arrive is None else arrive
-        span = parts[part]
+        span = return_parts[part]
         return send_to(
             summed.at[place, other, :, span],
             back.at[place, arrive, :, span],
@@ -256,15 +308,35 @@
                 move(upper, dsend, part, below).start()
 
     def choose(place, part):
-        span = gather_parts[part]
-        chosen = jnp.dot(pick[place], held[place, :, span], preferred_element_type=jnp.float32)
-        picked[place, :, :, span] = chosen.astype(low).reshape(
-            sp_count, slots, span.stop - span.start
-        )
+        span = parts[part]
+        base = gather_parts[part].start
+        inputs = held[place, :, span]
+        pick = one_hot(place, 0, slots, slots).astype(low)
+
+        def keep(value, start):
+            width = value.shape[1]
+            picked[place, :, :, start : start + width] = value.astype(low).reshape(
+                sp_count, slots, width
+            )
+
+        keep(jnp.dot(pick, inputs, preferred_element_type=jnp.float32), base)
+        if spare:
+            few = spare_hot(place).astype(low)
+            extra_rows = jnp.dot(few, inputs, preferred_element_type=jnp.float32).astype(low)
+            keep(fold(extra_rows), base + middle)
+        if part == 1:
+            tail = held[place, :, model:]
+            chosen = jnp.dot(pick, tail, preferred_element_type=jnp.float32)
+            if spare:
+                full = one_hot(place, slots, slots, spare).astype(low)
+                second = jnp.dot(full, tail, preferred_element_type=jnp.float32)
+                lane = lax.broadcasted_iota(jnp.int32, chosen.shape, 1)
+                chosen = jnp.where(lane < 64, chosen, second)
+            keep(chosen, 2 * sent)
         for other in others:
             spread(place, part, other).start()
         share(place, part, me, True).start()
-        rows[place, core, me, :, span] = picked[place, me, :, span]
+        rows[place, core, me, :, gather_parts[part]] = picked[place, me, :, gather_parts[part]]
 
     def relay(place, part):
         for other in others:
@@ -275,47 +347,96 @@
         for part in range(2):
             for source in range(sp_count):
                 shared(place, part, source).wait_recv()
-        x = rows[place].reshape(2 * sp_count * slots, wide)
-        inputs = x[:, :model]
-        tail = x[:, model:].astype(jnp.float32)
-        lane = lax.broadcasted_iota(jnp.int32, tail.shape, 1)
+        count = 2 * sp_count
+        full = count * slots
+
+        def stretch(start, width):
+            return rows[place, :, :, :, start : start + width].reshape(full, width)
+
+        inputs = []
+        for part in range(2):
+            x = stretch(part * sent, middle)
+            if spare:
+                few = unfold(stretch(part * sent + middle, segment))
+                x = jnp.concatenate([x, few], axis=0)
+            inputs.append(x)
+        tail = stretch(2 * sent, 128)
+        tails = [(tail.astype(jnp.float32), 0)]
+        if spare:
+            first = fold_matrix(0, count, False)
+            tails.append((jnp.dot(first, tail, preferred_element_type=jnp.float32), 64))
+
+        def scale_of(values, index):
+            lane = lax.broadcasted_iota(jnp.int32, values.shape, 1)
+            here = (lane == index) | (lane == index + experts * sp_count)
+            return jnp.sum(jnp.where(here, values, 0.0), axis=1, keepdims=True)
+
+        def expand(weight):
+            return jnp.dot(
+                inputs[0], weight[:middle], preferred_element_type=jnp.float32
+            ) + jnp.dot(inputs[1], weight[middle:], preferred_element_type=jnp.float32)
+
         hidden = []
         for e in range(experts):
             index = me * experts + e
-            here = (lane == index) | (lane == index + experts * sp_count)
-            scale = jnp.sum(jnp.where(here, tail, 0.0), axis=1, keepdims=True)
-            gate_out = jnp.dot(inputs, gate[e], preferred_element_type=jnp.float32)
-            up_out = jnp.dot(inputs, up[e], preferred_element_type=jnp.float32)
+            scale = [scale_of(values, index + start) for values, start in tails]
+            scale = jnp.concatenate(scale, axis=0) if spare else scale[0]
+            gate_out = expand(gate.at[e])
+            up_out = expand(up.at[e])
             hidden.append((jax.nn.silu(gate_out) * up_out * scale).astype(low))
         for part in range(2):
             span = parts[part]
             total = jnp.dot(hidden[0], down[0, :, span], preferred_element_type=jnp.float32)
             for e in range(1, experts):
                 total += jnp.dot(hidden[e], down[e, :, span], preferred_element_type=jnp.float32)
-            result[place, :, :, :, span] = total.astype(low).reshape(
-                2, sp_count, slots, span.stop - span.start
-            )
+            total = total.astype(low)
+            result[place, :, :, :, span] = total[:full].reshape(2, sp_count, slots, middle)
+            if spare:
+                result_spare[place, :, :, span] = total[full:].reshape(
+                    2, sp_count * spare, middle
+                )
+                swap_spare(place, part).start()
             swap(place, part).start()
 
     def settle(place, part):
         span = parts[part]
+        base = return_parts[part].start
         swap(place, part).wait_recv()
         kept = result[place, core, :, :, span].astype(jnp.float32)
         both = kept + swapped[place, :, :, span].astype(jnp.float32)
-        summed[place, :, :, span] = both.astype(low)
+        summed[place, :, :, base : base + middle] = both.astype(low)
+        if spare:
+            swap_spare(place, part).wait_recv()
+            kept = result_spare[place, core, :, span].astype(jnp.float32)
+            both = kept + swapped_spare[place, :, span].astype(jnp.float32)
+            summed[place, :, :, base + middle : base + sent] = fold(both.astype(low)).reshape(
+                sp_count, slots, segment
+            )
         for other in others:
             give(place, part, other).start()
-        back[place, me, :, span] = summed[place, me, :, span]
+        back[place, me, :, base : base + sent] = summed[place, me, :, base : base + sent]
 
     def combine(place, part):
         span = parts[part]
+        base = return_parts[part].start
         for other in others:
             give(place, part, other, other).wait_recv()
-        mixed[place, :, span] = jnp.dot(
-            back_pick[place],
-            back[place, :, :, span].reshape(sp_count * slots, span.stop - span.start),
+
+        def gathered(start, width):
+            return back[place, :, :, start : start + width].reshape(sp_count * slots, width)
+
+        total = jnp.dot(
+            one_hot(place, 0, slots, slots).T.astype(low),
+            gathered(base, middle),
             preferred_element_type=jnp.float32,
         )
+        if spare:
+            total += jnp.dot(
+                spare_hot(place).T.astype(low),
+                unfold(gathered(base + middle, segment)),
+                preferred_element_type=jnp.float32,
+            )
+        mixed[place, :, span] = total
 
         @pl.when((place > z) & (z == 0))
         def _():
@@ -425,6 +546,8 @@
                 give(place, part, other).wait_send()
             share(place, part, me, True).wait_send()
             swap(place, part).wait_send()
+            if spare:
+                swap_spare(place, part).wait_send()
         return unused
 
     lax.fori_loop(0, depth, finish, 0)
@@ -449,31 +572,41 @@
     tokens, model = residual.shape
     wide = model + extra.shape[1]
     low = residual.dtype
+    spare = slots % 8
+    fits = spare in (1, 2, 4) and slots - spare in (8, 16, 32, 64)
+    if fits and model // 2 * spare // (slots - spare) % 128 == 0:
+        slots = slots - spare
+    else:
+        spare = 0
+        slots = -(-slots // 8) * 8
+    sent = model // 2 * (slots + spare) // slots
     anywhere = pl.BlockSpec(memory_space=pl.ANY)
     each = dma((depth, sp_count, 2))
     two = dma((depth, 2))
     block = pltpu.VMEM((depth, tokens, model), low)
     group = pltpu.VMEM((depth, sp_count, slots, model), low)
+    carried = pltpu.VMEM((depth, sp_count, slots, 2 * sent), low)
+    few = max(spare * sp_count, 8)
     return pl.pallas_call(
-        functools.partial(moe_kernel, sp_count, tp_count),
+        functools.partial(moe_kernel, sp_count, tp_count, spare),
         out_shape=jax.ShapeDtypeStruct((tokens, model), low),
         in_specs=[VM, VM, VM, VM, VM, anywhere, anywhere, anywhere],
         out_specs=VM,
         scratch_shapes=[
             pltpu.VMEM((tokens, wide), low),
             pltpu.VMEM((tokens, model), jnp.float32),
-            pltpu.VMEM((depth, sp_count * slots, tokens), low),
-            pltpu.VMEM((depth, tokens, sp_count * slots), low),
             pltpu.VMEM((depth, tokens, wide), low),
-            pltpu.VMEM((depth, sp_count, slots, wide), low),
-            pltpu.VMEM((depth, 2, sp_count, slots, wide), low),
+            pltpu.VMEM((depth, sp_count, slots, 2 * sent + 128), low),
+            pltpu.VMEM((depth, 2, sp_count, slots, 2 * sent + 128), low),
             pltpu.VMEM(gate_weight.shape, gate_weight.dtype),
             pltpu.VMEM(up_weight.shape, up_weight.dtype),
             pltpu.VMEM(down_weight.shape, down_weight.dtype),
             pltpu.VMEM((depth, 2, sp_count, slots, model), low),
+            pltpu.VMEM((depth, 2, few, model), low),
             group,
-            group,
-            group,
+            pltpu.VMEM((depth, few, model), low),
+            carried,
+            carried,
             pltpu.VMEM((depth, tokens, model), jnp.float32),
             block,
             block,
@@ -485,6 +618,8 @@
             each,
             each,
             each,
+            two,
+            two,
             two,
             two,
             each,
@@ -567,8 +702,11 @@
             )
         )
     ]
-    for load in loads:
-        load.start()
+    loads[0].start()
+    met = greet_some(
+        [(True, partner), (has_above, above), (has_below, below)]
+        + [(True, (lax.rem(me + k, sp_count), tp)) for k in range(1, sp_count)]
+    )
     mine = pl.ds(pl.multiple_of(core * half, half), half)
     other = pl.ds(pl.multiple_of((1 - core) * half, half), half)
 
@@ -608,14 +746,13 @@
     rotated = list(rotate(raw[:turn], raw[turn:]))
     own[:, width:] = jnp.concatenate(rotated * (128 // rope_width), axis=0).T.astype(low)
     loads[0].wait()
+    for load in loads[1:]:
+        load.start()
     values = latent[...].astype(jnp.float32)
     inverse = lax.rsqrt(jnp.mean(values * values, axis=-1, keepdims=True) + epsilon)
     own[:, :width] = (values * inverse * gain_ref[...]).astype(low)
 
-    greet_some(
-        [(True, partner), (has_above, above), (has_below, below)]
-        + [(True, (lax.rem(me + k, sp_count), tp)) for k in range(1, sp_count)]
-    )
+    met()
     for to in reversed(range(sp_count)):
 
         @pl.when(to > me)
@@ -626,7 +763,7 @@
         lane = lax.broadcasted_iota(jnp.int32, one.shape, 1)
         return jnp.where(lane < DK_A, one, two)
 
-    for load in loads[1:]:
+    for load in loads[1:4]:
         load.wait()
     gap = jnp.zeros((DK_A - rope_width, tokens), jnp.float32)
     for pair in range(pairs):
@@ -747,6 +884,7 @@
             swap(place, part).start()
         return unused
 
+    loads[4].wait()
     lax.fori_loop(0, depth, project, 0)
 
     for j in range(depth - 1):
@@ -956,7 +1094,6 @@
     slots = experts_dev * capacity
     if experts_all // GROUPS == experts_dev == top_count:
         slots = capacity
-    slots = -(-slots // 8) * 8
     tp = lax.axis_index("tp")
     own = lax.dynamic_slice_in_dim(routes, tp * row_count, row_count, 0)
     route_weight = group_gate[:, None] * expert_share / jnp.sum(expert_share, axis=1, keepdims=True)
@@ -966,7 +1103,8 @@
     weight_high = table.astype(low)
     weight_low = (table - weight_high.astype(jnp.float32)).astype(low)
     extra = jnp.concatenate([weight_high, weight_low], axis=1)
-    extra = jnp.pad(extra, ((0, 0), (0, 128 - extra.shape[1])))
+    extra = jnp.pad(extra, ((0, 0), (0, 64 - extra.shape[1])))
+    extra = jnp.concatenate([extra, extra], axis=1)
 
     column = lax.dynamic_index_in_dim(
         routes.reshape(depth, 2, row_count, top_count), lax.rem(tp, 2), 1, keepdims=False

time: 108 us -> 104 us (0.963)
  Pallas kernels: 104 us -> 99.2 us
    pallas_call x1, Pallas kernels: 72.3 us -> 68.9 us  [moe(): pl.pallas_call(functools.partial(moe_kernel, sp_count, tp_count, spare),...]
    pallas_call x1, Pallas kernels: 31.6 us -> 30.4 us  [attend(): pl.pallas_call(functools.partial(attend_kernel, rope_width, sp_count, tp_...]
where the time goes in v3:
time: 104 us
  Pallas kernels  99.2 us (95%)
  local copies, waits for them, and re-layouts  1.91 us (2%)
  other arithmetic  1.55 us (1%)
    pallas_call x1, Pallas kernels, moe(): pl.pallas_call(functools.partial(moe_kernel, sp_count, tp_count, spare),...  68.9 us
    pallas_call x1, Pallas kernels, attend(): pl.pallas_call(functools.partial(attend_kernel, rope_width, sp_count, tp_...  30.4 us

profile of v3, /device:TPU:0, one launch (start us, length us, event | category | flops | bytes accessed | tf_op | source)
XLA Modules:
  0.0 103.5 jit_solution(18086310961206297053)
XLA Ops:
  0.0 0.0 copy-start.1
  0.0 0.0 copy-start.2
  0.0 0.0 copy-start
  0.0 0.8 multiply_sine_fusion
  0.8 30.4 %shard_map.154.heads_ref = f32[48,2048]{1,0:T(8,128)} custom-call(bf16[384,512]{1,0:T(8,128)(2,1)} %latent_ref.1, f32[1,512]{1,0:T(1,128)} %bitcast.21, bf16[32,384]{1,0:T(8,128)(2,1)} %bitcast.18, bf16[384,2,256]{2,1,0:T(2,128)(2,1)} %q_ref.1, bf16[2,64,384]{2,1,0:T(8,128)(2,1)} %bitcast.17, f32[16,384]{1,0:T(8,128)} %get-tuple-element.16.cos_ref, ...), custom_call_target="tpu_custom_call" | custom-call | tf_op jit(solution)/shard_map/pallas_call | solution.py:988
  31.2 0.0 copy-done
  31.2 0.1 constant_dynamic-slice_fusion.1
  31.3 0.0 copy-done.1
  31.3 0.0 copy-done.2
  31.4 0.1 copy.37
  31.5 0.7 pad_maximum_fusion.extra_ref
  32.2 0.1 reshape.52
  32.3 0.7 fusion.rank_ref
  33.1 68.9 %shard_map.155 = bf16[48,2048]{1,0:T(8,128)(2,1)} custom-call(f32[48,2048]{1,0:T(8,128)} %shard_map.154.heads_ref, bf16[48,2048]{1,0:T(8,128)(2,1)} %residual_ref.1, f32[1,2048]{1,0:T(1,128)} %bitcast.20, bf16[48,128]{1,0:T(8,128)(2,1)} %pad_maximum_fusion.extra_ref, s32[4,4,48]{2,1,0:T(4,128)} %fusion.rank_ref, bf16[2,2048,512]{2,1,0:T(8,128)(2,1)} %gate_ref.1, ...), custom_call_target="tpu_custom_call" | custom-call | tf_op jit(solution)/shard_map/pallas_call | solution.py:590
  101.9 1.6 %copy.42 = bf16[48,2048]{1,0:T(8,128)(2,1)} copy(bf16[48,2048]{1,0:T(8,128)(2,1)} %shard_map.155) | data formatting | bytes 393216
  (12 shorter events, 0.1 us)
Async XLA Ops:
  0.0 31.3 %copy-start.1 = (f32[48,2]{0,1:T(2,128)S(1)}, f32[48,2]{0,1:T(2,128)}, u32[]{:S(2)}) copy-start(f32[48,2]{0,1:T(2,128)} %param.28) | copy-start | bytes 1156
  0.0 31.3 %copy-start.2 = (f32[48]{0:T(128)S(1)}, f32[48]{0:T(128)}, u32[]{:S(2)}) copy-start(f32[48]{0:T(128)} %param.27) | copy-start | bytes 580
  0.0 31.2 %copy-start = (s32[384,2]{0,1:T(2,128)S(1)}, s32[384,2]{0,1:T(2,128)}, u32[]{:S(2)}) copy-start(s32[384,2]{0,1:T(2,128)} %param.26) | copy-start | bytes 9220

commit v4 on v3

--- a/solution.py
+++ b/solution.py
@@ -14,6 +14,7 @@
 rope_base = 10000.0
 epsilon = 1e-06
 floor_score = -1e30
+PIECES = 4
 MESH = pl.DeviceIdType.MESH
 VM = pl.BlockSpec(memory_space=pltpu.VMEM)
 
@@ -40,6 +41,17 @@
         device_id=target,
         device_id_type=MESH,
     )
+
+
+def grant(scratch, extra):
+    total = 0
+    for item in scratch:
+        if item.memory_space == pltpu.VMEM:
+            size = 1
+            for width in item.shape[:-1]:
+                size *= width
+            total += size * max(item.shape[-1], 128) * jnp.dtype(item.dtype).itemsize
+    return min(max(total // (1024 * 1024) + extra, 52), 60) * 1024 * 1024
 
 
 def greet_some(targets):
@@ -124,7 +136,10 @@
     middle = model // 2
     segment = middle * spare // slots
     sent = middle + segment
-    line_parts = (slice(0, middle), slice(middle, wide))
+    quarter = model // PIECES
+    hops = [slice(i * quarter, (i + 1) * quarter) for i in range(PIECES)]
+    line_parts = hops[:-1] + [slice(model - quarter, wide)]
+    share_of = PIECES // 2
     parts = (slice(0, middle), slice(middle, model))
     gather_parts = (slice(0, sent), slice(sent, rows.shape[4]))
     return_parts = (slice(0, sent), slice(sent, 2 * sent))
@@ -199,7 +214,7 @@
             target,
         )
 
-    for part in range(2):
+    for part in range(PIECES):
 
         @pl.when(has_above)
         def _():
@@ -275,8 +290,8 @@
 
     def pass_on(place, part, arrivals, sems, target):
         return remote(
-            stage.at[place, :, parts[part]],
-            arrivals.at[place, :, parts[part]],
+            stage.at[place, :, hops[part]],
+            arrivals.at[place, :, hops[part]],
             zsend.at[place, part],
             sems.at[place, part],
             target,
@@ -438,15 +453,18 @@
             )
         mixed[place, :, span] = total
 
-        @pl.when((place > z) & (z == 0))
-        def _():
-            stage[place, :, span] = mixed[place, :, span].astype(low)
-            rise(place, part).start()
-
-        @pl.when((place < z) & (z == depth - 1))
-        def _():
-            stage[place, :, span] = mixed[place, :, span].astype(low)
-            fall(place, part).start()
+        for hop in range(part * share_of, (part + 1) * share_of):
+            span = hops[hop]
+
+            @pl.when((place > z) & (z == 0))
+            def _():
+                stage[place, :, span] = mixed[place, :, span].astype(low)
+                rise(place, hop).start()
+
+            @pl.when((place < z) & (z == depth - 1))
+            def _():
+                stage[place, :, span] = mixed[place, :, span].astype(low)
+                fall(place, hop).start()
 
     def at(k, action):
         def one(side, unused):
@@ -464,7 +482,8 @@
         @pl.when(t < depth)
         def _():
             for part in range(2):
-                take(t, part)
+                for piece in range(part * share_of, (part + 1) * share_of):
+                    take(t, piece)
                 at(t, lambda place: choose(place, part))
 
         @pl.when(t == 1)
@@ -483,8 +502,8 @@
     def hop(key, unused):
         high = key - z
         deep = 2 * depth - 2 - key - z
-        for part in range(2):
-            span = parts[part]
+        for part in range(PIECES):
+            span = hops[part]
 
             @pl.when((high > z) & (high < depth) & has_below)
             def _():
@@ -505,8 +524,8 @@
         return unused
 
     lax.fori_loop(1, 2 * depth - 2, hop, 0)
-    for part in range(2):
-        span = parts[part]
+    for part in range(PIECES):
+        span = hops[part]
         token_rows[:, span] += mixed[z, :, span]
 
         @pl.when(has_below)
@@ -522,24 +541,25 @@
         out_ref[:, span] = token_rows[:, span].astype(low)
 
     def finish(place, unused):
+        for part in range(PIECES):
+
+            @pl.when(has_above & (place <= z))
+            def _():
+                move(place, usend, part, above).wait_send()
+
+            @pl.when(has_below & (place >= z))
+            def _():
+                move(place, dsend, part, below).wait_send()
+
+            @pl.when(place > z)
+            def _():
+                rise(place, part).wait_send()
+
+            @pl.when(place < z)
+            def _():
+                fall(place, part).wait_send()
+
         for part in range(2):
-
-            @pl.when(has_above & (place <= z))
-            def _():
-                move(place, usend, part, above).wait_send()
-
-            @pl.when(has_below & (place >= z))
-            def _():
-                move(place, dsend, part, below).wait_send()
-
-            @pl.when(place > z)
-            def _():
-                rise(place, part).wait_send()
-
-            @pl.when(place < z)
-            def _():
-                fall(place, part).wait_send()
-
             for other in others:
                 spread(place, part, other).wait_send()
                 share(place, part, other).wait_send()
@@ -583,54 +603,56 @@
     anywhere = pl.BlockSpec(memory_space=pl.ANY)
     each = dma((depth, sp_count, 2))
     two = dma((depth, 2))
+    fine = dma((depth, PIECES))
     block = pltpu.VMEM((depth, tokens, model), low)
     group = pltpu.VMEM((depth, sp_count, slots, model), low)
     carried = pltpu.VMEM((depth, sp_count, slots, 2 * sent), low)
     few = max(spare * sp_count, 8)
+    scratch = [
+        pltpu.VMEM((tokens, wide), low),
+        pltpu.VMEM((tokens, model), jnp.float32),
+        pltpu.VMEM((depth, tokens, wide), low),
+        pltpu.VMEM((depth, sp_count, slots, 2 * sent + 128), low),
+        pltpu.VMEM((depth, 2, sp_count, slots, 2 * sent + 128), low),
+        pltpu.VMEM(gate_weight.shape, gate_weight.dtype),
+        pltpu.VMEM(up_weight.shape, up_weight.dtype),
+        pltpu.VMEM(down_weight.shape, down_weight.dtype),
+        pltpu.VMEM((depth, 2, sp_count, slots, model), low),
+        pltpu.VMEM((depth, 2, few, model), low),
+        group,
+        pltpu.VMEM((depth, few, model), low),
+        carried,
+        carried,
+        pltpu.VMEM((depth, tokens, model), jnp.float32),
+        block,
+        block,
+        block,
+        fine,
+        fine,
+        fine,
+        each,
+        each,
+        each,
+        each,
+        two,
+        two,
+        two,
+        two,
+        each,
+        each,
+        fine,
+        fine,
+        fine,
+        dma((3,)),
+    ]
     return pl.pallas_call(
         functools.partial(moe_kernel, sp_count, tp_count, spare),
         out_shape=jax.ShapeDtypeStruct((tokens, model), low),
         in_specs=[VM, VM, VM, VM, VM, anywhere, anywhere, anywhere],
         out_specs=VM,
-        scratch_shapes=[
-            pltpu.VMEM((tokens, wide), low),
-            pltpu.VMEM((tokens, model), jnp.float32),
-            pltpu.VMEM((depth, tokens, wide), low),
-            pltpu.VMEM((depth, sp_count, slots, 2 * sent + 128), low),
-            pltpu.VMEM((depth, 2, sp_count, slots, 2 * sent + 128), low),
-            pltpu.VMEM(gate_weight.shape, gate_weight.dtype),
-            pltpu.VMEM(up_weight.shape, up_weight.dtype),
-            pltpu.VMEM(down_weight.shape, down_weight.dtype),
-            pltpu.VMEM((depth, 2, sp_count, slots, model), low),
-            pltpu.VMEM((depth, 2, few, model), low),
-            group,
-            pltpu.VMEM((depth, few, model), low),
-            carried,
-            carried,
-            pltpu.VMEM((depth, tokens, model), jnp.float32),
-            block,
-            block,
-            block,
-            two,
-            two,
-            two,
-            each,
-            each,
-            each,
-            each,
-            two,
-            two,
-            two,
-            two,
-            each,
-            each,
-            two,
-            two,
-            two,
-            dma((3,)),
-        ],
+        scratch_shapes=scratch,
         compiler_params=pltpu.CompilerParams(
-            collective_id=identity, has_side_effects=True, vmem_limit_bytes=60 * 1024 * 1024
+            collective_id=identity, has_side_effects=True, vmem_limit_bytes=grant(scratch, 8)
         ),
     )(heads, residual, norm_gain[None, :], extra, rank, gate_weight, up_weight, down_weight)
 
@@ -783,6 +805,12 @@
     ]
     splits = ((slice(0, 128), slice(0, DV_A)), (slice(128, None), slice(DV_A, pair_width)))
 
+    def ahead(index):
+        @pl.when(index >= 0)
+        def _():
+            incoming(index).wait_recv()
+            forward(index).start()
+
     def block(index, first):
         source = own if first else held.at[index]
         compressed = source[:, :width]
@@ -796,6 +824,8 @@
                 wvt[pair], compressed, NT, preferred_element_type=jnp.float32
             ).astype(low)
         for pair in range(pairs):
+            if pair == 1 and not first:
+                ahead(index - 1)
             for group, (span, part) in enumerate(splits):
                 head = pair * 2 + group
                 scores = lax.dot_general(
@@ -824,11 +854,10 @@
                     acc[pair, part] = acc[pair, part] * factor + update
 
     block(me, True)
+    ahead(me - 1)
 
     def step(i, unused):
         index = me - 1 - i
-        incoming(index).wait_recv()
-        forward(index).start()
         forwarded(index).wait_recv()
         block(index, False)
         return unused
@@ -840,8 +869,8 @@
         attention[:, pair * pair_width : (pair + 1) * pair_width] = acc[pair].T.astype(low)
 
     row_count, model = out_ref.shape
-    middle = model // 256 * 128
-    parts = (slice(0, middle), slice(middle, model))
+    quarter = model // PIECES
+    parts = [slice(i * quarter, (i + 1) * quarter) for i in range(PIECES)]
 
     def swap(place, part):
         return remote(
@@ -877,7 +906,7 @@
         place = turnabout * (n // 2) + (1 - turnabout) * (depth - 1 - n // 2)
         rows = pl.ds(pl.multiple_of(place * 2 * row_count, 2 * row_count), 2 * row_count)
         inputs = attention[rows]
-        for part in range(2):
+        for part in range(PIECES):
             mixed = jnp.dot(inputs, wo[:, parts[part]], preferred_element_type=jnp.float32)
             mixed = mixed.astype(low).reshape(2, row_count, mixed.shape[1])
             partial[pl.ds(place * 2, 2), :, parts[part]] = mixed
@@ -889,7 +918,7 @@
 
     for j in range(depth - 1):
         high, deep = depth - 1 + z - j, j + z + 1 - depth
-        for part in range(2):
+        for part in range(PIECES):
             span = parts[part]
 
             @pl.when(z <= j)
@@ -920,7 +949,7 @@
 
                 down(deep, part).start()
 
-    for part in range(2):
+    for part in range(PIECES):
         span = parts[part]
         out_ref[:, span] = pair_sum(z, part)
 
@@ -945,7 +974,7 @@
             outgoing(place).wait_send()
 
     for place in range(depth):
-        for part in range(2):
+        for part in range(PIECES):
             swap(place, part).wait_send()
 
             @pl.when(place > z)
@@ -985,43 +1014,44 @@
     padded = pair_width + 128
     anywhere = pl.BlockSpec(memory_space=pl.ANY)
     block = vmem((depth, row_count, model), low)
+    scratch = [
+        vmem(latent.shape, low),
+        vmem(queries.shape, low),
+        vmem(key_weight.shape, low),
+        vmem(value_weight.shape, low),
+        vmem(out_weight.shape, low),
+        vmem((tokens, latent_width + 128), low),
+        vmem((sp_count, tokens, latent_width + 128), low),
+        vmem((pairs, tokens, padded), low),
+        vmem((pairs, latent_width, pair_width), low),
+        vmem((pairs, pair_width, latent_width), low),
+        vmem((pairs, tokens, padded), low),
+        vmem((pairs, pair_width, tokens), low),
+        vmem((2 * pairs, 1, tokens), f32),
+        vmem((2 * pairs, 1, tokens), f32),
+        vmem((pairs, pair_width, tokens), f32),
+        vmem((tokens, pairs * pair_width), low),
+        vmem((tp_count, row_count, model), low),
+        block,
+        block,
+        block,
+        block,
+        dma((5,)),
+        dma((sp_count,)),
+        dma((sp_count, 2)),
+        dma((sp_count,)),
+        dma((depth, PIECES)),
+        dma((depth, PIECES)),
+        dma((depth, PIECES)),
+        dma((depth, PIECES)),
+        dma((depth, PIECES)),
+    ]
     return pl.pallas_call(
         functools.partial(attend_kernel, rope_width, sp_count, tp_count),
         out_shape=jax.ShapeDtypeStruct((row_count, model), f32),
         in_specs=[anywhere, VM, VM, anywhere, VM, VM, VM, anywhere, anywhere, anywhere],
         out_specs=VM,
-        scratch_shapes=[
-            vmem(latent.shape, low),
-            vmem(queries.shape, low),
-            vmem(key_weight.shape, low),
-            vmem(value_weight.shape, low),
-            vmem(out_weight.shape, low),
-            vmem((tokens, latent_width + 128), low),
-            vmem((sp_count, tokens, latent_width + 128), low),
-            vmem((pairs, tokens, padded), low),
-            vmem((pairs, latent_width, pair_width), low),
-            vmem((pairs, pair_width, latent_width), low),
-            vmem((pairs, tokens, padded), low),
-            vmem((pairs, pair_width, tokens), low),
-            vmem((2 * pairs, 1, tokens), f32),
-            vmem((2 * pairs, 1, tokens), f32),
-            vmem((pairs, pair_width, tokens), f32),
-            vmem((tokens, pairs * pair_width), low),
-            vmem((tp_count, row_count, model), low),
-            block,
-            block,
-            block,
-            block,
-            dma((5,)),
-            dma((sp_count,)),
-            dma((sp_count, 2)),
-            dma((sp_count,)),
-            dma((depth, 2)),
-            dma((depth, 2)),
-            dma((depth, 2)),
-            dma((depth, 2)),
-            dma((depth, 2)),
-        ],
+        scratch_shapes=scratch,
         compiler_params=pltpu.CompilerParams(
             collective_id=identity, has_side_effects=True, vmem_limit_bytes=60 * 1024 * 1024
         ),

time: 104 us -> 99.9 us (0.961)
  Pallas kernels: 99.2 us -> 96.5 us
    pallas_call x1, Pallas kernels: 68.9 us -> 66.3 us  [moe(): pl.pallas_call(functools.partial(moe_kernel, sp_count, tp_count, spare),...]
where the time goes in v4:
time: 99.9 us; the launch traced here: 99.7 us
  Pallas kernels  96.5 us (97%)
  local copies, waits for them, and re-layouts  1.97 us (2%)
    pallas_call x1, Pallas kernels, moe(): pl.pallas_call(functools.partial(moe_kernel, sp_count, tp_count, spare),...  66.3 us
    pallas_call x1, Pallas kernels, attend(): pl.pallas_call(functools.partial(attend_kernel, rope_width, sp_count, tp_...  30.2 us

profile of v4, /device:TPU:0, one launch (start us, length us, event | category | flops | bytes accessed | tf_op | source)
XLA Modules:
  0.0 99.7 jit_solution(16835410362685106635)
XLA Ops:
  0.0 0.0 copy-start.4
  0.0 0.0 copy-start.5
  0.0 0.0 copy-start.3
  0.0 0.0 copy-start.2
  0.0 0.0 copy-start.1
  0.1 0.8 multiply_sine_fusion
  0.8 30.2 %shard_map.154.heads_ref = f32[48,2048]{1,0:T(8,128)} custom-call(bf16[384,512]{1,0:T(8,128)(2,1)} %latent_ref.1, f32[1,512]{1,0:T(1,128)} %bitcast.21, bf16[32,384]{1,0:T(8,128)(2,1)} %bitcast.19, bf16[384,2,256]{2,1,0:T(2,128)(2,1)} %q_ref.1, bf16[2,64,384]{2,1,0:T(8,128)(2,1)} %bitcast.18, f32[16,384]{1,0:T(8,128)} %get-tuple-element.16.cos_ref, ...), custom_call_target="tpu_custom_call" | custom-call | tf_op jit(solution)/shard_map/pallas_call | solution.py:1049
  31.0 0.0 copy-done.3
  31.0 0.1 constant_dynamic-slice_fusion.1
  31.1 0.0 copy-done.4
  31.2 0.0 copy-done.5
  31.2 0.1 copy.37
  31.3 0.1 pad_maximum_fusion.extra_ref
  31.4 0.1 reshape.52
  31.6 0.1 fusion.rank_ref
  31.7 0.0 copy-done.2
  31.7 0.0 copy-done.1
  31.7 0.0 copy-start
  31.7 1.0 copy-done
  32.7 66.3 %shard_map.155 = bf16[48,2048]{1,0:T(8,128)(2,1)S(1)} custom-call(f32[48,2048]{1,0:T(8,128)S(1)} %copy-done, bf16[48,2048]{1,0:T(8,128)(2,1)S(1)} %copy-done.1, f32[1,2048]{1,0:T(1,128)S(1)} %bitcast.16, bf16[48,128]{1,0:T(8,128)(2,1)S(1)} %pad_maximum_fusion.extra_ref, s32[4,4,48]{2,1,0:T(4,128)S(1)} %fusion.rank_ref, bf16[2,2048,512]{2,1,0:T(8,128)(2,1)} %gate_ref.1, ...), custom_call_target="tpu_custom_call" | custom-call | tf_op jit(solution)/shard_map/pallas_call | solution.py:648
  99.0 0.7 copy.42
  (12 shorter events, 0.1 us)
Async XLA Ops:
  0.0 31.1 %copy-start.4 = (f32[48,2]{0,1:T(2,128)S(1)}, f32[48,2]{0,1:T(2,128)}, u32[]{:S(2)}) copy-start(f32[48,2]{0,1:T(2,128)} %param.28) | copy-start | bytes 1156
  0.0 31.2 %copy-start.5 = (f32[48]{0:T(128)S(1)}, f32[48]{0:T(128)}, u32[]{:S(2)}) copy-start(f32[48]{0:T(128)} %param.27) | copy-start | bytes 580
  0.0 31.0 %copy-start.3 = (s32[384,2]{0,1:T(2,128)S(1)}, s32[384,2]{0,1:T(2,128)}, u32[]{:S(2)}) copy-start(s32[384,2]{0,1:T(2,128)} %param.26) | copy-start | bytes 9220
  0.0 31.7 %copy-start.2 = (f32[2048]{0:T(1024)S(1)}, f32[2048]{0:T(1024)}, u32[]{:S(2)}) copy-start(f32[2048]{0:T(1024)} %param.25) | copy-start | bytes 24580
  0.0 31.7 %copy-start.1 = (bf16[48,2048]{1,0:T(8,128)(2,1)S(1)}, bf16[48,2048]{1,0:T(8,128)(2,1)}, u32[]{:S(2)}) copy-start(bf16[48,2048]{1,0:T(8,128)(2,1)} %residual_ref.1) | copy-start | bytes 589828
  31.7 1.0 copy-start
